TPU v7x, 256 devices: a whole 4x4x8 slice. The times are simulated.
256 devices in a mesh: ep: 128 (over z, y, x), tp: 2 (over core).
Axes of the slice: x: 4, y: 4, z: 8, core: 2. Of those that a mesh axis runs over, the one named last changes fastest.
Arguments:
- stream: bfloat16 [2048, 2048], P('ep', 'tp'), may hold values from -6 to 6
- hidden_state: float32 [2048, 2048], P('ep', 'tp'), may hold values from -6 to 6
- conv_state: bfloat16 [2048, 3, 2048], P('ep', None, 'tp'), may hold values from -6 to 6
- first_gain: float32 [2048], P('tp'), may hold values from 0.1 to 1.9
- input_weight: bfloat16 [2048, 2048], P('tp', 'ep'), may hold values from -0.125 to 0.125
- branch_weight: bfloat16 [2048, 2048], P('tp', 'ep'), may hold values from -0.125 to 0.125
- conv_taps: bfloat16 [4, 2048], P(None, 'tp'), may hold values from -3 to 3
- recur_gate: bfloat16 [32, 64, 64], P('tp'), may hold values from -0.75 to 0.75
- input_gate: bfloat16 [32, 64, 64], P('tp'), may hold values from -0.75 to 0.75
- decay_logit: float32 [2048], P('tp'), may hold values from 1.5 to 8
- output_weight: bfloat16 [2048, 2048], P('tp', 'ep'), may hold values from -0.25 to 0.25
- second_gain: float32 [2048], P('tp'), may hold values from 0.1 to 1.9
- routes: int32 [2048, 2], P('ep'), may hold values from 0 to 31, all different within a row; in each aligned block of 16 rows (0 to 15, 16 to 31, ...) at most 2 rows name the same one
- route_weight: float32 [2048, 2], P('ep'), may hold values from 0.25 to 1
- expert_gate: bfloat16 [2048, 98304], P(None, ('ep', 'tp')), may hold values from -0.125 to 0.125
- expert_up: bfloat16 [2048, 98304], P(None, ('ep', 'tp')), may hold values from -0.125 to 0.125
- expert_down: bfloat16 [98304, 2048], P(('ep', 'tp')), may hold values from -0.21875 to 0.21875
Outputs:
- new_stream: bfloat16 [2048, 2048], P('ep', 'tp')
- new_hidden: float32 [2048, 2048], P('ep', 'tp')
- new_conv: bfloat16 [2048, 3, 2048], P('ep', None, 'tp')
Inputs may be any that keep to these rules, and one draw needn't show every extreme that they name: `routes`: among the rows of one index of ep, no expert is named more than 2 times; in every draw some expert is named exactly 2 times by the rows of some index. Each row names different experts.
All inputs are finite; a program needn't handle non-finite values.
Results may differ from a plain program's by a relative error of at most 0.022.
Values may be sent and summed in bfloat16 or wider, within the bound.
A program may use at most 128 MiB of HBM per device.

v0:
```python
import jax
import jax.numpy as jnp
from jax import lax
from jax.sharding import Mesh
from jax.sharding import PartitionSpec as P

EP_SPAN = 4
EP = ("ep_0", "ep_1", "ep_2")
EP_TP = ("ep_0", "ep_1", "ep_2", "tp")


epsilon = 1e-06
decay_power = 8.0


def gather_turned(arrays, axis, dims):
    turned = [jnp.moveaxis(a, dim, 0) for a, dim in zip(arrays, dims)]
    both = jnp.concatenate([t.reshape(len(t), -1) for t in turned], axis=1)
    filled, at, finished = (lax.all_gather(both, axis, axis=0, tiled=True), 0, [])
    for t, dim in zip(turned, dims):
        section = filled[:, at : at + t[0].size].reshape(-1, *t.shape[1:])
        finished.append(jnp.moveaxis(section, 0, dim))
        at += t[0].size
    return tuple(finished)


def in_blocks(x, dim, size):
    before, after = (x.shape[:dim], x.shape[dim + 1 :])
    return jnp.moveaxis(x.reshape(*before, size, -1, *after), dim, 0)


def sum_at_owner(x, axis, dim):
    parts = in_blocks(x, dim, lax.axis_size(axis))
    arrived = lax.all_to_all(parts, axis, split_axis=0, concat_axis=0, tiled=True)
    return arrived.astype(jnp.float32).sum(axis=0)


def gathered_by_axis(x, axes, dim):
    for axis in reversed(axes):
        x = lax.all_gather(x, axis, axis=dim, tiled=True)
    return x


def gathered_total(x, axis):
    parts = lax.all_gather(x, axis)
    return parts.sum(axis=0)


def joined_along(parts, dim):
    parts = jnp.moveaxis(parts, 0, dim)
    shape = parts.shape
    return parts.reshape(*shape[:dim], shape[dim] * shape[dim + 1], *shape[dim + 2 :])


def copy_for_each(x, axis):
    size = lax.axis_size(axis)
    return lax.all_to_all(jnp.broadcast_to(x[None], (size, *x.shape)), axis, 0, 0, tiled=True)


def gather_directly(x, axis, dim):
    return joined_along(copy_for_each(x, axis), dim)


def block_map(values, table):
    seq_count = values.shape[0]
    heads, inner_width, _ = table.shape
    split = values.reshape(seq_count, heads, inner_width)
    mapped = jnp.einsum("shi,hij->shj", split, table, preferred_element_type=jnp.float32)
    return mapped.reshape(seq_count, heads * inner_width)


def per_device(
    stream,
    hidden_state,
    conv_state,
    first_gain,
    input_weight,
    branch_weight,
    conv_taps,
    recur_gate,
    input_gate,
    decay_logit,
    output_weight,
    second_gain,
    routes,
    route_weight,
    expert_gate,
    expert_up,
    expert_down,
):
    seq_dev, half_width = stream.shape
    tp_count = lax.axis_size("tp")
    model_width = half_width * tp_count
    values = stream.astype(jnp.float32)
    square_sum = jnp.sum(values * values, axis=1)
    scaled = (values * first_gain).astype(jnp.bfloat16)
    column_block = jnp.einsum(
        "nd,dsc->nsc",
        scaled,
        jnp.stack(gather_turned((input_weight, branch_weight), EP, (1, 1)), axis=1),
        preferred_element_type=jnp.float32,
    )
    partial_terms = column_block
    square_terms = jnp.broadcast_to(square_sum[:, None, None], (seq_dev, 1, tp_count))
    partial_terms, square_terms = (
        sum_at_owner(partial_terms.astype(jnp.bfloat16), "tp", 2),
        sum_at_owner(square_terms.astype(jnp.bfloat16), "tp", 2),
    )
    row_scale = lax.rsqrt(square_terms / model_width + epsilon)
    projected = (partial_terms * row_scale).astype(jnp.bfloat16)
    forward = projected[:, 0]
    branch = projected[:, 1]
    window = jnp.concatenate([conv_state, forward[:, None, :]], axis=1)
    new_conv = window[:, 1:]
    conv_out = jnp.einsum(
        "skc,kc->sc", window.astype(jnp.float32), conv_taps.astype(jnp.float32)
    ).astype(jnp.bfloat16)
    recur_open = jax.nn.sigmoid(block_map(conv_out, recur_gate))
    inward = jax.nn.sigmoid(block_map(conv_out, input_gate))
    log_decay = -decay_power * recur_open * jax.nn.softplus(-decay_logit)
    new_hidden = jnp.exp(log_decay) * hidden_state + jnp.sqrt(-jnp.expm1(2.0 * log_decay)) * (
        inward * conv_out.astype(jnp.float32)
    )
    mixed_rows = (jax.nn.gelu(branch.astype(jnp.float32)) * new_hidden).astype(jnp.bfloat16)
    out_terms = jnp.dot(
        mixed_rows, gathered_by_axis(output_weight, EP, 1), preferred_element_type=jnp.float32
    )
    out_terms = sum_at_owner(out_terms.astype(jnp.bfloat16), "tp", 1)
    middle = (values + out_terms).astype(jnp.bfloat16)
    mid_values = middle.astype(jnp.float32)
    mean_square = gathered_total(jnp.sum(mid_values * mid_values, axis=1), "tp")
    normed = (
        mid_values * lax.rsqrt(mean_square / model_width + epsilon)[:, None] * second_gain
    ).astype(jnp.bfloat16)
    experts = lax.axis_size(EP) // EP_SPAN
    top_count = routes.shape[1]
    capacity = max(2, 2 * seq_dev * top_count // experts)
    flat_routes = routes.reshape(-1)
    expert_hits = (flat_routes[:, None] == jnp.arange(experts, dtype=jnp.int32)[None, :]).astype(
        jnp.int32
    )
    slot_rank = jnp.sum((jnp.cumsum(expert_hits, axis=0) - expert_hits) * expert_hits, axis=1)
    target = flat_routes * capacity + slot_rank
    picking = target[:, None] == jnp.arange(experts * capacity, dtype=jnp.int32)[None, :]
    repeated = jnp.repeat(normed, top_count, axis=0)
    buffer = jnp.einsum(
        "ae,ad->ed", picking.astype(jnp.bfloat16), repeated, preferred_element_type=jnp.float32
    ).astype(jnp.bfloat16)
    buffer = buffer.reshape(experts, capacity, normed.shape[1])
    outgoing = jnp.repeat(buffer, EP_SPAN, axis=0)
    slot_rows = gather_directly(
        lax.all_to_all(outgoing, EP, split_axis=0, concat_axis=0, tiled=True), "tp", 2
    )
    sources, slot_count, _ = slot_rows.shape
    flat_rows = slot_rows.reshape(sources * slot_count, model_width)
    gate_act = jnp.dot(flat_rows, expert_gate, preferred_element_type=jnp.float32)
    upper = jnp.dot(flat_rows, expert_up, preferred_element_type=jnp.float32)
    inner_act = (jax.nn.silu(gate_act) * upper).astype(jnp.bfloat16)
    partial_value = jnp.dot(inner_act, expert_down, preferred_element_type=jnp.float32)
    partial_value = sum_at_owner(partial_value.astype(jnp.bfloat16), "tp", 1)
    partial_value = partial_value.reshape(sources, slot_count, half_width)
    returned = lax.all_to_all(
        partial_value.astype(jnp.bfloat16), EP, split_axis=0, concat_axis=0, tiled=True
    ).astype(partial_value.dtype)
    summed = jnp.sum(returned.reshape(experts, EP_SPAN, capacity, half_width), axis=1).reshape(
        experts * capacity, half_width
    )
    picked = jnp.dot(
        picking.astype(jnp.float32),
        summed,
        precision=lax.Precision.HIGHEST,
        preferred_element_type=jnp.float32,
    )
    expert_mix = jnp.sum(
        picked.reshape(seq_dev, top_count, half_width) * route_weight[:, :, None], axis=1
    )
    new_stream = (mid_values + expert_mix).astype(jnp.bfloat16)
    return (new_stream, new_hidden, new_conv)


def solution(mesh):
    torus = Mesh(mesh.devices.reshape(8, 4, 4, mesh.shape["tp"]), ("ep_0", "ep_1", "ep_2", "tp"))
    in_specs = (
        P(EP, "tp"),
        P(EP, "tp"),
        P(EP, None, "tp"),
        P("tp"),
        P("tp", EP),
        P("tp", EP),
        P(None, "tp"),
        P("tp", None, None),
        P("tp", None, None),
        P("tp"),
        P("tp", EP),
        P("tp"),
        P(EP, None),
        P(EP, None),
        P(None, EP_TP),
        P(None, EP_TP),
        P(EP_TP, None),
    )
    out_specs = (P(EP, "tp"), P(EP, "tp"), P(EP, None, "tp"))
    return jax.shard_map(
        per_device, mesh=torus, in_specs=in_specs, out_specs=out_specs, check_vma=False
    )
```

profile of v0, /device:TPU:2, one launch (start us, length us, event | category | flops | bytes accessed | tf_op | source)
XLA Modules:
  0.0 289.4 jit_solution(2138599489067912806)
XLA Ops:
  7.2 1.5 pad_maximum_fusion.1
  8.8 12.3 %all_gather.19 = bf16[1024,64]{0,1:T(8,128)(2,1)S(1)} all-gather(bf16[1024,16]{0,1:T(8,128)(2,1)} %param.27), channel_id=1, replica_groups=mesh['ep_0'=8,'ep_1'=4,'ep_2'=4,'tp'=2] {'ep_2'}, dimensions={1}, use_global_device_ids=true | all-gather | bytes 163840 | tf_op jit(solution)/shard_map/all_gather | solution.py:40
  21.1 14.5 %all_gather.20 = bf16[1024,256]{0,1:T(8,128)(2,1)} all-gather(bf16[1024,64]{0,1:T(8,128)(2,1)S(1)} %all_gather.19), channel_id=1, replica_groups=mesh['ep_0'=8,'ep_1'=4,'ep_2'=4,'tp'=2] {'ep_1'}, dimensions={1}, use_global_device_ids=true | all-gather | bytes 655360 | tf_op jit(solution)/shard_map/all_gather | solution.py:40
  35.6 0.9 fusion.26
  36.5 0.6 transpose.76
  37.1 3.2 %all-to-all-start.1 = ((bf16[2,16,1,1]{1,3,2,0:T(2,128)(2,1)}), bf16[2,16,1,1]{1,3,2,0:T(2,128)(2,1)S(1)}, u32[]{:S(2)}, u32[]{:S(2)}) async-start(bf16[2,16,1,1]{1,3,2,0:T(2,128)(2,1)} %transpose.76), calls=%async_computation.1 | async-start | bytes 2048 | tf_op jit(solution)/shard_map/all_to_all | solution.py:34
  40.3 0.8 copy.90
  41.2 1.3 dynamic-slice
  43.4 0.7 fusion.54
  44.1 0.7 bitcast_convert_fusion
  44.8 94.4 %all-gather.4.cloned.1.call-done = bf16[2048,2048]{1,0:T(8,128)(2,1)} async-done(((bf16[16,2048]{1,0:T(8,128)(2,1)}), bf16[2048,2048]{1,0:T(8,128)(2,1)}) %all-gather.4.cloned.1.call-update) | async-done | bytes 8388624 | tf_op jit(solution)/shard_map/all_gather | solution.py:19
  139.2 5.9 %fusion.62 = (bf16[2048,1024]{1,0:T(8,128)(2,1)}, bf16[2048,1024]{1,0:T(8,128)(2,1)}) fusion(bf16[2048,2048]{1,0:T(8,128)(2,1)} %all-gather.4.cloned.1.call-done), kind=kLoop, calls=%fused_computation.99 | loop fusion | bytes 16777216 | tf_op jit(solution)/shard_map/slice | solution.py:21
  145.2 6.5 %copy.103 = bf16[2048,1024]{0,1:T(8,128)(2,1)} copy(bf16[2048,1024]{1,0:T(8,128)(2,1)} %get-tuple-element.5) | data formatting | bytes 8388608
  151.7 6.5 %copy.104 = bf16[2048,1024]{0,1:T(8,128)(2,1)} copy(bf16[2048,1024]{1,0:T(8,128)(2,1)} %get-tuple-element.6) | data formatting | bytes 8388608
  158.3 4.3 %fusion.4 = bf16[16,2,2048]{2,0,1:T(8,128)(2,1)S(1)} fusion(bf16[1024,1,2048]{2,0,1:T(8,128)(2,1)} %bitcast.77, bf16[1024,1,2048]{2,0,1:T(8,128)(2,1)} %bitcast.76, bf16[16,1024]{1,0:T(8,128)(2,1)S(1)} %copy-done.4, f32[1024]{0:T(1024)S(1)} %copy-done.11), kind=kOutput, calls=%fused_computation.5 | convolution fusion | flops 151109632 | bytes 8556544 | tf_op jit(solution)/shard_map/nd,dsc->nsc/dot_general | solution.py:97
  162.6 3.8 %all_to_all.35 = bf16[2,16,2,1024]{3,1,2,0:T(8,128)(2,1)S(1)} all-to-all(bf16[2,16,2,1024]{3,1,2,0:T(8,128)(2,1)S(1)} %bitcast.83), channel_id=1, replica_groups=mesh['ep_0'=8,'ep_1'=4,'ep_2'=4,'tp'=2] {'tp'}, dimensions={0} | all-to-all | bytes 262144 | tf_op jit(solution)/shard_map/all_to_all | solution.py:34
  167.5 25.2 %all-gather.6.cloned.1.call-done = bf16[1024,2048]{0,1:T(8,128)(2,1)} async-done(((bf16[1024,256]{0,1:T(8,128)(2,1)}), bf16[1024,2048]{0,1:T(8,128)(2,1)}) %all-gather.6.cloned.1.call-update) | async-done | bytes 4194320 | tf_op jit(solution)/shard_map/all_gather | solution.py:40
  192.7 3.4 %convolution_convert_fusion.1 = bf16[16,2048]{1,0:T(8,128)(2,1)S(1)} fusion(bf16[1024,2048]{0,1:T(8,128)(2,1)} %all-gather.6.cloned.1.call-done, f32[16,1024]{1,0:T(8,128)S(1)} %multiply_add_fusion, bf16[16,2,1024]{2,0,1:T(8,128)(2,1)S(1)} %multiply_convert_fusion), kind=kOutput, calls=%fused_computation.6 | convolution fusion | flops 67321856 | bytes 4358144 | tf_op jit(solution)/shard_map/dot_general | solution.py:125
  196.1 3.8 %all_to_all.36 = bf16[2,16,1024]{2,1,0:T(8,128)(2,1)S(1)} all-to-all(bf16[2,16,1024]{2,1,0:T(8,128)(2,1)S(1)} %bitcast.86), channel_id=1, replica_groups=mesh['ep_0'=8,'ep_1'=4,'ep_2'=4,'tp'=2] {'tp'}, dimensions={0} | all-to-all | bytes 131072 | tf_op jit(solution)/shard_map/all_to_all | solution.py:34
  200.3 2.4 all-reduce
  203.6 31.3 %all_to_all.37 = bf16[128,2,1024]{2,1,0:T(2,128)(2,1)S(1)} all-to-all(bf16[128,2,1024]{2,1,0:T(2,128)(2,1)S(1)} %bitcast.81), channel_id=1, replica_groups=mesh['ep_0'=8,'ep_1'=4,'ep_2'=4,'tp'=2] {'ep_0','ep_1','ep_2'}, dimensions={0} | all-to-all | bytes 1048576 | tf_op jit(solution)/shard_map/all_to_all | solution.py:152
  235.5 4.6 %all_to_all.38 = bf16[2,128,2,1024]{3,2,1,0:T(2,128)(2,1)S(1)} all-to-all(bf16[2,128,2,1024]{3,2,1,0:T(2,128)(2,1)S(1)} %broadcast_in_dim.8), channel_id=1, replica_groups=mesh['ep_0'=8,'ep_1'=4,'ep_2'=4,'tp'=2] {'tp'}, dimensions={0} | all-to-all | bytes 2097152 | tf_op jit(solution)/shard_map/all_to_all | solution.py:57
  240.1 1.6 copy.92
  242.0 0.7 fusion.63
  242.7 3.7 %convolution_convert_fusion = bf16[256,2048]{1,0:T(8,128)(2,1)} fusion(bf16[384,2048]{1,0:T(8,128)(2,1)S(1)} %copy-done, bf16[256,2048]{1,0:T(8,128)(2,1)S(1)} %bitcast.75, bf16[2048,384]{1,0:T(8,128)(2,1)} %param.32, f32[256,384]{1,0:T(8,128)S(1)} %fusion.63), kind=kOutput, calls=%fused_computation.4 | convolution fusion | flops 806420480 | bytes 5636096 | tf_op jit(solution)/shard_map/dot_general | solution.py:159
  246.5 1.3 copy.118
  247.8 4.6 %all_to_all.39 = bf16[2,256,1024]{2,1,0:T(8,128)(2,1)S(1)} all-to-all(bf16[2,256,1024]{2,1,0:T(8,128)(2,1)S(1)} %bitcast.80), channel_id=1, replica_groups=mesh['ep_0'=8,'ep_1'=4,'ep_2'=4,'tp'=2] {'tp'}, dimensions={0} | all-to-all | bytes 2097152 | tf_op jit(solution)/shard_map/all_to_all | solution.py:34
  252.6 1.0 convert_element_type.107
  253.6 6.6 %all-to-all-start.6 = ((bf16[128,2,1024]{2,1,0:T(2,128)(2,1)}), bf16[128,2,1024]{2,1,0:T(2,128)(2,1)S(1)}, u32[]{:S(2)}, u32[]{:S(2)}) async-start(bf16[128,2,1024]{2,1,0:T(2,128)(2,1)} %convert_element_type.107), calls=%async_computation.6 | async-start | bytes 1048576 | tf_op jit(solution)/shard_map/all_to_all | solution.py:162
  260.4 0.7 fusion.24
  261.1 19.8 %all-to-all-done.6 = bf16[128,2,1024]{2,1,0:T(2,128)(2,1)S(1)} async-done(((bf16[128,2,1024]{2,1,0:T(2,128)(2,1)}), bf16[128,2,1024]{2,1,0:T(2,128)(2,1)S(1)}, u32[]{:S(2)}, u32[]{:S(2)}) %all-to-all-start.6) | async-done | bytes 524320 | tf_op jit(solution)/shard_map/all_to_all | solution.py:162
  281.9 0.6 fusion.31
  (72 shorter events, 5.1 us)
Async XLA Ops:
  7.2 235.5 %copy-start = (bf16[384,2048]{1,0:T(8,128)(2,1)S(1)}, bf16[384,2048]{1,0:T(8,128)(2,1)}, u32[]{:S(2)}) copy-start(bf16[384,2048]{1,0:T(8,128)(2,1)} %param.33) | copy-start | bytes 4718596
  7.2 132.1 %all-gather.4.cloned.1.call-start = ((), (), s32[]{:S(2)}) async-start(), calls=%async_computation.7 | async-start | bytes 8454144 | tf_op jit(solution)/shard_map/all_gather | solution.py:19
  8.8 183.9 %all-gather.6.cloned.1.call-start = ((), (), s32[]{:S(2)}) async-start(), calls=%async_computation.8 | async-start | bytes 4718592 | tf_op jit(solution)/shard_map/all_gather | solution.py:40
  37.1 6.1 %all-to-all-start.1 = ((bf16[2,16,1,1]{1,3,2,0:T(2,128)(2,1)}), bf16[2,16,1,1]{1,3,2,0:T(2,128)(2,1)S(1)}, u32[]{:S(2)}, u32[]{:S(2)}) async-start(bf16[2,16,1,1]{1,3,2,0:T(2,128)(2,1)} %transpose.76), calls=%async_computation.1 | async-start | bytes 2048 | tf_op jit(solution)/shard_map/all_to_all | solution.py:34
  151.7 6.6 %copy-start.4 = (bf16[16,1024]{1,0:T(8,128)(2,1)S(1)}, bf16[16,1024]{1,0:T(8,128)(2,1)}, u32[]{:S(2)}) copy-start(bf16[16,1024]{1,0:T(8,128)(2,1)} %param.17) | copy-start | bytes 98308
  151.7 6.6 %copy-start.11 = (f32[1024]{0:T(1024)S(1)}, f32[1024]{0:T(1024)}, u32[]{:S(2)}) copy-start(f32[1024]{0:T(1024)} %param.20) | copy-start | bytes 12292
  158.2 8.3 %copy-start.2 = (bf16[16,3,1024]{2,0,1:T(8,128)(2,1)S(1)}, bf16[16,3,1024]{2,0,1:T(8,128)(2,1)}, u32[]{:S(2)}) copy-start(bf16[16,3,1024]{2,0,1:T(8,128)(2,1)} %param.19) | copy-start | bytes 294916
  158.2 8.4 %copy-start.9 = (bf16[16,64,64]{2,1,0:T(8,128)(2,1)S(1)}, bf16[16,64,64]{2,1,0:T(8,128)(2,1)}, u32[]{:S(2)}) copy-start(bf16[16,64,64]{2,1,0:T(8,128)(2,1)} %param.24) | copy-start | bytes 393220
  158.2 8.8 %copy-start.10 = (bf16[16,64,64]{2,1,0:T(8,128)(2,1)S(1)}, bf16[16,64,64]{2,1,0:T(8,128)(2,1)}, u32[]{:S(2)}) copy-start(bf16[16,64,64]{2,1,0:T(8,128)(2,1)} %param.25) | copy-start | bytes 393220
  158.3 9.1 %copy-start.5 = (f32[16,1024]{1,0:T(8,128)S(1)}, f32[16,1024]{1,0:T(8,128)}, u32[]{:S(2)}) copy-start(f32[16,1024]{1,0:T(8,128)} %param.18) | copy-start | bytes 196612
  166.4 36.4 %copy-start.6 = (f32[1024]{0:T(1024)S(1)}, f32[1024]{0:T(1024)}, u32[]{:S(2)}) copy-start(f32[1024]{0:T(1024)} %param.28) | copy-start | bytes 12292
  167.5 68.0 %copy-start.3 = (f32[16,1024]{1,0:T(8,128)}, f32[16,1024]{1,0:T(8,128)S(1)}, u32[]{:S(2)}) copy-start(f32[16,1024]{1,0:T(8,128)S(1)} %multiply_add_fusion) | copy-start | bytes 196612
  234.9 7.0 %copy-start.1 = (bf16[2048,384]{1,0:T(8,128)(2,1)S(1)}, bf16[2048,384]{1,0:T(8,128)(2,1)}, u32[]{:S(2)}) copy-start(bf16[2048,384]{1,0:T(8,128)(2,1)} %param.31) | copy-start | bytes 4718596
  246.5 14.0 %copy-start.7 = (s32[16,2]{0,1:T(2,128)S(1)}, s32[16,2]{0,1:T(2,128)}, u32[]{:S(2)}) copy-start(s32[16,2]{0,1:T(2,128)} %param.29) | copy-start | bytes 388
  246.5 35.2 %copy-start.8 = (f32[16,2]{0,1:T(2,128)S(1)}, f32[16,2]{0,1:T(2,128)}, u32[]{:S(2)}) copy-start(f32[16,2]{0,1:T(2,128)} %param.30) | copy-start | bytes 388
  253.6 27.3 %all-to-all-start.6 = ((bf16[128,2,1024]{2,1,0:T(2,128)(2,1)}), bf16[128,2,1024]{2,1,0:T(2,128)(2,1)S(1)}, u32[]{:S(2)}, u32[]{:S(2)}) async-start(bf16[128,2,1024]{2,1,0:T(2,128)(2,1)} %convert_element_type.107), calls=%async_computation.6 | async-start | bytes 1048576 | tf_op jit(solution)/shard_map/all_to_all | solution.py:162
Sparse Core Ops, SparseCore 0:
  12.2 127.0 all-gather.3
  141.0 51.6 all-gather.5
where the time goes:
time: 290 us; the launch traced here: 289 us
  waiting for transfers between devices  139 us (48%)
  blocking collectives  77.3 us (27%)
  local copies, waits for them, and re-layouts  27.9 us (10%)
  between operations  15 us (5%)
  matrix products  13.1 us (5%)
  starting transfers between devices  9.9 us (3%)
  other arithmetic  6.64 us (2%)
    all_gather x1, waiting for transfers between devices, gather_turned(): lax.all_gather(both, axis, axis=0, tiled=True)  94.4 us
    all_to_all x1, blocking collectives, per_device(): lax.all_to_all(outgoing, EP, split_axis=0, concat_axis=0, tiled=True)  31.3 us
    all_gather x2, blocking collectives, gathered_by_axis(): x = lax.all_gather(x, axis, axis=dim, tiled=True)  26.8 us
    all_gather x1, waiting for transfers between devices, gathered_by_axis(): x = lax.all_gather(x, axis, axis=dim, tiled=True)  25.2 us
    all_to_all x1, waiting for transfers between devices, per_device(): lax.all_to_all(partial_value.astype(jnp.bfloat16), EP, split_axis=0, conc...  19.8 us
    unnamed x31, local copies, waits for them, and re-layouts  15.6 us
    all_to_all x3, blocking collectives, sum_at_owner(): lax.all_to_all(parts, axis, split_axis=0, concat_axis=0, tiled=True)  12.2 us
    all_to_all x1, starting transfers between devices, per_device(): lax.all_to_all(partial_value.astype(jnp.bfloat16), EP, split_axis=0, conc...  6.62 us
  transfers between devices with their start and end apart: 4, of which 3 were waited for; matrix products, arithmetic and copies ran while one was open for 10% of the time, Pallas kernels for 0%

commit v1 on v0

v1 whole, which is shorter than its diff:
```python
import jax
import jax.numpy as jnp
from jax import lax
from jax.experimental import pallas as pl
from jax.experimental.pallas import tpu as pltpu
from jax.sharding import Mesh
from jax.sharding import PartitionSpec as P

EP = ("z", "y", "x")
EP_TP = ("z", "y", "x", "tp")
MESH = pl.DeviceIdType.MESH
NZ, NY, NX = 8, 4, 4
ORDER = {8: (1, 7, 2, 6, 3, 5, 4), 4: (1, 3, 2)}
BF, F32 = jnp.bfloat16, jnp.float32
EPSILON = 1e-6
DECAY_POWER = 8.0
S, H, D, FD = 16, 1024, 2048, 384
LANES, Q = 128, 8
EXPERTS, CAP = 32, 2
HIGHEST = lax.Precision.HIGHEST


def scratch_shapes():
    vm, dma = pltpu.VMEM, pltpu.SemaphoreType.DMA
    return dict(
        sv=vm((S, H), BF),
        hv=vm((S, H), F32),
        cv=vm((3, S, H), BF),
        g1v=vm((1, H), F32),
        tv=vm((4, H), BF),
        rgv=vm((H, 64), BF),
        igv=vm((H, 64), BF),
        dv=vm((1, H), F32),
        g2v=vm((1, H), F32),
        rtv=vm((2, S), jnp.int32),
        rwv=vm((2, S), F32),
        wg=vm((Q, 2, LANES, FD), BF),
        wu=vm((Q, 2, LANES, FD), BF),
        wd=vm((FD, D), BF),
        xs=vm((NZ, S, H), BF),
        ms=vm((NZ, S, H), BF),
        wt=vm((3, 4, 4, S, H), BF),
        ps=vm((NZ * S, 512), BF),
        pr=vm((NZ * S, 512), BF),
        ss=vm((NZ, S, 512), BF),
        ra=vm((4, S, 512), BF),
        ps2=vm((NZ * S, 256), BF),
        pr2=vm((NZ * S, 256), BF),
        ss2=vm((NZ, S, 256), BF),
        rb=vm((4, S, 256), BF),
        qs=vm((2, S, LANES), F32),
        qr=vm((2, S, LANES), F32),
        bd=vm((2, 4, 256, 256), BF),
        pm=vm((EXPERTS * 16, LANES), BF),
        pw=vm((EXPERTS * 16, LANES), F32),
        zsend=vm((NZ, NY, 16, LANES), BF),
        zrecv=vm((NZ, NY, 16, LANES), BF),
        fb=vm((2, NX, NY, NZ, 16, LANES), BF),
        ab=vm((256, D), BF),
        ib=vm((256, FD), BF),
        hs=vm((NX, 64, H), BF),
        hr=vm((NX, 64, H), BF),
        own=vm((NX, 64, H), F32),
        xsend=vm((NX, 64, H), BF),
        xrecv=vm((NX, 64, H), BF),
        ysend=vm((NY, NZ, 16, LANES), BF),
        ry=vm((NY, NZ, 16, LANES), BF),
        rz=vm((NZ, NY, 16, LANES), BF),
        nh=vm((S, H), F32),
        nc=vm((3, S, H), BF),
        ns=vm((S, H), BF),
        loads=dma((24,)),
        stores=dma((3,)),
        x_s=dma((8,)), x_r=dma((8,)),
        m_s=dma((8,)), m_r=dma((8,)),
        w1_s=dma((2, 4)), w1_r=dma((2, 4)),
        w2_s=dma((2, 4)), w2_r=dma((2, 4)),
        t_s=dma((4,)), t_r=dma((4,)),
        a_s=dma((8,)), a_r=dma((4,)),
        b_s=dma((8,)), b_r=dma((4,)),
        dz_s=dma((8,)), dz_r=dma((8,)),
        dy_s=dma((4,)), dy_r=dma((4,)),
        dx_s=dma((4,)), dx_r=dma((4,)),
        dt_s=dma((4,)), dt_r=dma((4,)),
        ht_s=dma((4,)), ht_r=dma((4,)),
        rx_s=dma((4,)), rx_r=dma((4,)),
        ry_s=dma((4,)), ry_r=dma((4,)),
        rz_s=dma((8,)), rz_r=dma((8,)),
    )


NAMES = tuple(scratch_shapes())


def dot(a, b, dims=((1,), (0,)), precision=None):
    return lax.dot_general(a, b, (dims, ((), ())), precision=precision, preferred_element_type=F32)


def iota(shape, dim):
    return lax.broadcasted_iota(jnp.int32, shape, dim)


def expm1(v):
    series = 1.0 + v * (1.0 / 9.0)
    for n in range(8, 1, -1):
        series = 1.0 + v * (1.0 / n) * series
    return jnp.where(v > -0.5, v * series, jnp.exp(v) - 1.0)


def remote(src, dst, ssem, rsem, where):
    return pltpu.make_async_remote_copy(
        src_ref=src, dst_ref=dst, send_sem=ssem, recv_sem=rsem, device_id=where, device_id_type=MESH
    )


def kernel(*refs):
    (stream, hidden, conv, gain1, w_in, w_br, taps, rg, ig, decay, w_out, gain2, routes, rw, eg, eu, ed) = refs[:17]
    o_stream, o_hidden, o_conv = refs[17:20]
    k = dict(zip(NAMES, refs[20:]))
    z, y, x, tp = (lax.axis_index(a) for a in EP_TP)
    other = 1 - tp
    sent = []

    barrier = pltpu.get_barrier_semaphore()
    for axis, me in (("z", z), ("y", y), ("x", x)):
        n = {"z": NZ, "y": NY, "x": NX}[axis]
        for d in ORDER[n]:
            pl.semaphore_signal(barrier, inc=1, device_id={axis: lax.rem(me + d, n)}, device_id_type=MESH)
    pl.semaphore_signal(barrier, inc=1, device_id={"tp": other}, device_id_type=MESH)

    a = y + tp * (x - y)
    b = x + tp * (y - x)
    plan = [
        (stream, k["sv"]), (gain1, k["g1v"]),
        (w_in, k["wt"].at[0, a, b]), (w_br, k["wt"].at[1, a, b]), (w_out, k["wt"].at[2, a, b]),
        (rg, k["rgv"]), (ig, k["igv"]), (routes, k["rtv"]), (rw, k["rwv"]),
        (conv, k["cv"]), (taps, k["tv"]), (decay, k["dv"]), (hidden, k["hv"]), (gain2, k["g2v"]),
        (eg.at[0], k["wg"].at[:, 0]), (eg.at[1], k["wg"].at[:, 1]),
        (eu.at[0], k["wu"].at[:, 0]), (eu.at[1], k["wu"].at[:, 1]), (ed, k["wd"]),
    ]
    loads = [pltpu.make_async_copy(s, t, k["loads"].at[i]) for i, (s, t) in enumerate(plan)]
    for c in loads:
        c.start()

    def start(src, dst, ssem, rsem, where):
        c = remote(src, dst, ssem, rsem, where)
        c.start()
        sent.append(c)

    def await_recv(ref, ssem, rsem, where):
        remote(ref, ref, ssem, rsem, where).wait_recv()

    loads[0].wait()
    loads[1].wait()
    values = k["sv"][...].astype(F32)
    k["xs"][z] = (values * k["g1v"][...]).astype(BF)
    k["qs"][0] = jnp.broadcast_to(jnp.sum(values * values, axis=1, keepdims=True), (S, LANES))
    for i in (2, 3, 4):
        loads[i].wait()
    pl.semaphore_wait(barrier, 14)

    for kinds, n in ((pl.ds(0, 2), 0), (pl.ds(2, 1), 1)):
        for d in ORDER[4]:
            there = {"y": lax.rem(y + d * tp, NY), "x": lax.rem(x + d * other, NX)}
            block = k["wt"].at[kinds, a, b]
            start(block, block, k["w1_s"].at[n, d], k["w1_r"].at[n, d], there)
        if n == 0:
            for d in ORDER[8]:
                start(k["xs"].at[z], k["xs"].at[z], k["x_s"].at[d], k["x_r"].at[d], {"z": lax.rem(z + d, NZ)})
            start(k["qs"].at[0], k["qr"].at[0], k["t_s"].at[0], k["t_r"].at[0], {"tp": other})

    def second_stage(kinds, n):
        for d in ORDER[4]:
            block = k["wt"].at[kinds, a, lax.rem(b - d + 4, 4)]
            await_recv(block, k["w1_s"].at[n, d], k["w1_r"].at[n, d], {"tp": other})
        for d in ORDER[4]:
            there = {"y": lax.rem(y + d * other, NY), "x": lax.rem(x + d * tp, NX)}
            block = k["wt"].at[kinds, a]
            start(block, block, k["w2_s"].at[n, d], k["w2_r"].at[n, d], there)

    def second_arrived(kinds, n):
        for d in ORDER[4]:
            block = k["wt"].at[kinds, lax.rem(a - d + 4, 4)]
            await_recv(block, k["w2_s"].at[n, d], k["w2_r"].at[n, d], {"tp": other})

    second_stage(pl.ds(0, 2), 0)

    loads[5].wait()
    loads[6].wait()
    eye = (iota((64, 256), 1) % 64 == iota((64, 256), 0)).astype(BF)
    on = iota((H, 256), 0) // 64 % 4 == iota((H, 256), 1) // 64
    for n, ref in enumerate((k["rgv"], k["igv"])):
        k["bd"][n] = jnp.where(on, dot(ref[...], eye), 0.0).astype(BF).reshape(4, 256, 256)

    loads[7].wait()
    loads[8].wait()
    spread = (iota((S, LANES), 1) % S == iota((S, LANES), 0)).astype(F32)
    named = dot(k["rtv"][...].astype(F32), spread, precision=HIGHEST)
    weights = dot(k["rwv"][...], spread, precision=HIGHEST)
    rows = (EXPERTS * 16, LANES)
    expert = (iota(rows, 0) // 16).astype(F32)
    hit0, hit1 = named[0:1] == expert, named[1:2] == expert
    hits = jnp.where(hit0 | hit1, 1.0, 0.0)
    square = (LANES, LANES)
    before = (iota(square, 0) < iota(square, 1) % S).astype(BF)
    rank = dot(hits.astype(BF), before)
    slot = (iota(rows, 0) // Q % CAP).astype(F32)
    chosen = (hits > 0.5) & (rank == slot) & (iota(rows, 0) % Q == iota(rows, 1) // S)
    k["pm"][...] = jnp.where(chosen, 1.0, 0.0).astype(BF)
    k["pw"][...] = jnp.where(chosen, jnp.where(hit0, weights[0:1], weights[1:2]), 0.0)

    second_stage(pl.ds(2, 1), 1)
    for d in ORDER[8]:
        await_recv(k["xs"].at[lax.rem(z - d + NZ, NZ)], k["x_s"].at[d], k["x_r"].at[d], {"tp": other})
    second_arrived(pl.ds(0, 2), 0)

    def columns(kind):
        blocks = []
        for i in range(4):
            for j in range(4):
                blocks.append(k["wt"][kind, i + tp * (j - i), j + tp * (i - j)])
        return jnp.concatenate(blocks, axis=0)

    def project(rows_ref, kinds, width, ps, pr, ss, land, t, sends, lands):
        lhs = k[rows_ref][...].reshape(NZ * S, H)
        part = jnp.concatenate([dot(lhs, columns(kind), ((1,), (1,))) for kind in kinds], axis=1)

        @pl.when(tp != z // 4)
        def _():
            k[ps][...] = part.astype(BF)
            c = remote(k[ps], k[pr], k["t_s"].at[t], k["t_r"].at[t], {"tp": other})
            c.start()
            c.wait_send()

        @pl.when(tp == z // 4)
        def _():
            await_recv(k[pr], k["t_s"].at[t], k["t_r"].at[t], {"tp": other})
            total = (part + k[pr][...].astype(F32)).astype(BF)
            k[ss][...] = total.reshape(NZ, S, width)
            mine = lax.rem(z, 4)
            for d in ORDER[8]:
                there = lax.rem(z + d, NZ)
                remote(k[ss].at[there], k[land].at[mine], k[sends].at[d], k[lands].at[mine], {"z": there}).start()
            k[land][mine] = k[ss][z]

        for i in range(4):
            @pl.when(4 * tp + i != z)
            def _():
                await_recv(k[land].at[i], k[sends].at[0], k[lands].at[i], {"tp": other})

    def sends_done(ss, land, sends, lands):
        @pl.when(tp == z // 4)
        def _():
            for d in ORDER[8]:
                remote(k[ss].at[0], k[land].at[0], k[sends].at[d], k[lands].at[0], {"tp": other}).wait_send()

    project("xs", (0, 1), 512, "ps", "pr", "ss", "ra", 1, "a_s", "a_r")
    await_recv(k["qr"].at[0], k["t_s"].at[0], k["t_r"].at[0], {"tp": other})
    row_scale = lax.rsqrt((k["qs"][0] + k["qr"][0])[:, 0:1] / D + EPSILON)
    forward = (jnp.concatenate([k["ra"][i, :, 0:256] for i in range(4)], axis=1).astype(F32) * row_scale).astype(BF)
    branch = (jnp.concatenate([k["ra"][i, :, 256:512] for i in range(4)], axis=1).astype(F32) * row_scale).astype(BF)
    for i in range(9, 14):
        loads[i].wait()
    window = [k["cv"][0], k["cv"][1], k["cv"][2], forward]
    k["nc"][0] = window[1]
    k["nc"][1] = window[2]
    k["nc"][2] = forward
    store_conv = pltpu.make_async_copy(k["nc"], o_conv, k["stores"].at[0])
    store_conv.start()
    tap_rows = k["tv"][...].astype(F32)
    conv_out = sum(window[i].astype(F32) * tap_rows[i : i + 1] for i in range(4)).astype(BF)

    def gate_map(n):
        return jnp.concatenate([dot(conv_out[:, g * 256 : g * 256 + 256], k["bd"][n, g]) for g in range(4)], axis=1)

    recur_open = jax.nn.sigmoid(gate_map(0))
    inward = jax.nn.sigmoid(gate_map(1))
    logit = -k["dv"][...]
    softplus = jnp.maximum(logit, 0.0) + jnp.log1p(jnp.exp(-jnp.abs(logit)))
    log_decay = -DECAY_POWER * recur_open * softplus
    new_hidden = jnp.exp(log_decay) * k["hv"][...] + jnp.sqrt(-expm1(2.0 * log_decay)) * (
        inward * conv_out.astype(F32)
    )
    k["nh"][...] = new_hidden
    store_hidden = pltpu.make_async_copy(k["nh"], o_hidden, k["stores"].at[1])
    store_hidden.start()
    k["ms"][z] = (jax.nn.gelu(branch.astype(F32)) * new_hidden).astype(BF)
    for d in ORDER[8]:
        start(k["ms"].at[z], k["ms"].at[z], k["m_s"].at[d], k["m_r"].at[d], {"z": lax.rem(z + d, NZ)})
    second_arrived(pl.ds(2, 1), 1)
    for d in ORDER[8]:
        await_recv(k["ms"].at[lax.rem(z - d + NZ, NZ)], k["m_s"].at[d], k["m_r"].at[d], {"tp": other})
    project("ms", (2,), 256, "ps2", "pr2", "ss2", "rb", 2, "b_s", "b_r")
    out_terms = jnp.concatenate([k["rb"][i] for i in range(4)], axis=1).astype(F32)
    middle = (values + out_terms).astype(BF)
    mid_values = middle.astype(F32)
    k["qs"][1] = jnp.broadcast_to(jnp.sum(mid_values * mid_values, axis=1, keepdims=True), (S, LANES))
    start(k["qs"].at[1], k["qr"].at[1], k["t_s"].at[3], k["t_r"].at[3], {"tp": other})
    await_recv(k["qr"].at[1], k["t_s"].at[3], k["t_r"].at[3], {"tp": other})
    mid_scale = lax.rsqrt((k["qs"][1] + k["qr"][1])[:, 0:1] / D + EPSILON)
    normed = (mid_values * mid_scale * k["g2v"][...]).astype(BF)

    stacked = jnp.concatenate([normed[:, q * LANES : (q + 1) * LANES] for q in range(Q)], axis=0)
    k["zsend"][...] = dot(k["pm"][...], stacked).astype(BF).reshape(NZ, NY, 16, LANES)
    for d in ORDER[8]:
        there = lax.rem(z + d, NZ)
        start(k["zsend"].at[there], k["zrecv"].at[z], k["dz_s"].at[d], k["dz_r"].at[d], {"z": there})
    k["zrecv"][z] = k["zsend"][z]
    for d in ORDER[8]:
        await_recv(k["zrecv"].at[lax.rem(z - d + NZ, NZ)], k["dz_s"].at[d], k["dz_r"].at[d], {"tp": other})
    for d in ORDER[4]:
        there = lax.rem(y + d, NY)
        start(k["zrecv"].at[:, there], k["fb"].at[tp, x, y], k["dy_s"].at[d], k["dy_r"].at[d], {"y": there})
    k["fb"][tp, x, y] = k["zrecv"][:, y]
    for d in ORDER[4]:
        block = k["fb"].at[tp, x, lax.rem(y - d + NY, NY)]
        await_recv(block, k["dy_s"].at[d], k["dy_r"].at[d], {"tp": other})
    for d in ORDER[4]:
        there = lax.rem(x + d, NX)
        start(k["fb"].at[tp, x], k["fb"].at[tp, x], k["dx_s"].at[d], k["dx_r"].at[d], {"x": there})
    for d in (0,) + ORDER[4]:
        block = k["fb"].at[tp, lax.rem(x - d + NX, NX)]
        if d:
            await_recv(block, k["dx_s"].at[d], k["dx_r"].at[d], {"tp": other})
        start(block, block, k["dt_s"].at[d], k["dt_r"].at[d], {"tp": other})
    for i in range(14, 19):
        loads[i].wait()
    for d in (0,) + ORDER[4]:
        block = k["fb"].at[other, lax.rem(x - d + NX, NX)]
        await_recv(block, k["dt_s"].at[d], k["dt_r"].at[d], {"tp": other})

    turn = iota(square, 1) == iota(square, 0) % 16 * Q + iota(square, 0) // 16
    turn = jnp.where(turn, 1.0, 0.0).astype(BF)
    for g in range(NX * NY):
        pair = jnp.concatenate([k["fb"][h, g // NY, g % NY].reshape(LANES, LANES) for h in range(2)], axis=1)
        turned = dot(turn, pair).astype(BF)
        for q in range(Q):
            k["ab"][g * 16 : g * 16 + 16, q * 256 : q * 256 + 256] = turned[q * 16 : q * 16 + 16]
    gate_act = dot(k["ab"][...], k["wg"][...].reshape(D, FD))
    upper = dot(k["ab"][...], k["wu"][...].reshape(D, FD))
    k["ib"][...] = (jax.nn.silu(gate_act) * upper).astype(BF)

    for d in ORDER[4] + (0,):
        there = lax.rem(x + d, NX)
        inner = k["ib"][pl.ds(pl.multiple_of(there * 64, 64), 64)]
        theirs = pl.ds(pl.multiple_of(other * H, H), H)
        ours = pl.ds(pl.multiple_of(tp * H, H), H)
        k["hs"][there] = dot(inner, k["wd"][:, theirs]).astype(BF)
        start(k["hs"].at[there], k["hr"].at[there], k["ht_s"].at[d], k["ht_r"].at[d], {"tp": other})
        k["own"][there] = dot(inner, k["wd"][:, ours])
    for d in ORDER[4] + (0,):
        there = lax.rem(x + d, NX)
        await_recv(k["hr"].at[there], k["ht_s"].at[d], k["ht_r"].at[d], {"tp": other})
        whole = k["own"][there] + k["hr"][there].astype(F32)
        if d:
            k["xsend"][there] = whole.astype(BF)
            start(k["xsend"].at[there], k["xrecv"].at[x], k["rx_s"].at[d], k["rx_r"].at[d], {"x": there})
    for d in ORDER[4]:
        source = lax.rem(x - d + NX, NX)
        await_recv(k["xrecv"].at[source], k["rx_s"].at[d], k["rx_r"].at[d], {"tp": other})
        whole = whole + k["xrecv"][source].astype(F32)
    whole = whole.astype(BF)
    back = iota(square, 0) == iota(square, 1) % 16 * Q + iota(square, 1) // 16
    back = jnp.where(back, 1.0, 0.0).astype(BF)
    for g in range(NY):
        part = whole[g * 16 : g * 16 + 16]
        part = jnp.concatenate([part[:, q * LANES : (q + 1) * LANES] for q in range(Q)], axis=0)
        k["ysend"][g] = dot(back, part).astype(BF).reshape(NZ, 16, LANES)
    for d in ORDER[4]:
        there = lax.rem(y + d, NY)
        start(k["ysend"].at[there], k["ry"].at[y], k["ry_s"].at[d], k["ry_r"].at[d], {"y": there})
    k["ry"][y] = k["ysend"][y]
    for d in ORDER[4]:
        await_recv(k["ry"].at[lax.rem(y - d + NY, NY)], k["ry_s"].at[d], k["ry_r"].at[d], {"tp": other})
    for d in ORDER[8]:
        there = lax.rem(z + d, NZ)
        start(k["ry"].at[:, there], k["rz"].at[z], k["rz_s"].at[d], k["rz_r"].at[d], {"z": there})
    k["rz"][z] = k["ry"][:, z]
    for d in ORDER[8]:
        await_recv(k["rz"].at[lax.rem(z - d + NZ, NZ)], k["rz_s"].at[d], k["rz_r"].at[d], {"tp": other})
    returned = k["rz"][...].reshape(EXPERTS * 16, LANES).astype(F32)
    mix = dot(k["pw"][...], returned, ((0,), (0,)), HIGHEST)
    expert_mix = jnp.concatenate([mix[q * S : (q + 1) * S] for q in range(Q)], axis=1)
    k["ns"][...] = (mid_values + expert_mix).astype(BF)
    store_stream = pltpu.make_async_copy(k["ns"], o_stream, k["stores"].at[2])
    store_stream.start()

    for c in sent:
        c.wait_send()
    sends_done("ss", "ra", "a_s", "a_r")
    sends_done("ss2", "rb", "b_s", "b_r")
    store_conv.wait()
    store_hidden.wait()
    store_stream.wait()


def per_device(
    stream, hidden_state, conv_state, first_gain, input_weight, branch_weight, conv_taps, recur_gate, input_gate,
    decay_logit, output_weight, second_gain, routes, route_weight, expert_gate, expert_up, expert_down,
):
    shapes = scratch_shapes()
    anywhere = pl.BlockSpec(memory_space=pl.ANY)
    outs = pl.pallas_call(
        kernel,
        name="layer",
        out_shape=(
            jax.ShapeDtypeStruct((S, H), BF),
            jax.ShapeDtypeStruct((S, H), F32),
            jax.ShapeDtypeStruct((3, S, H), BF),
        ),
        in_specs=[anywhere] * 17,
        out_specs=(anywhere,) * 3,
        scratch_shapes=[shapes[n] for n in NAMES],
        compiler_params=pltpu.CompilerParams(
            collective_id=0, has_side_effects=True, vmem_limit_bytes=60 * 1024 * 1024
        ),
    )(
        stream,
        hidden_state,
        conv_state.transpose(1, 0, 2),
        first_gain.reshape(1, H),
        input_weight.T,
        branch_weight.T,
        conv_taps,
        recur_gate.reshape(H, 64),
        input_gate.reshape(H, 64),
        decay_logit.reshape(1, H),
        output_weight.T,
        second_gain.reshape(1, H),
        routes.T,
        route_weight.T,
        expert_gate.reshape(2, Q, LANES, FD),
        expert_up.reshape(2, Q, LANES, FD),
        expert_down,
    )
    new_stream, new_hidden, new_conv = outs
    return new_stream, new_hidden, new_conv.transpose(1, 0, 2)


def solution(mesh):
    torus = Mesh(mesh.devices.reshape(NZ, NY, NX, mesh.shape["tp"]), EP_TP)
    in_specs = (
        P(EP, "tp"),
        P(EP, "tp"),
        P(EP, None, "tp"),
        P("tp"),
        P("tp", EP),
        P("tp", EP),
        P(None, "tp"),
        P("tp", None, None),
        P("tp", None, None),
        P("tp"),
        P("tp", EP),
        P("tp"),
        P(EP, None),
        P(EP, None),
        P(None, EP_TP),
        P(None, EP_TP),
        P(EP_TP, None),
    )
    out_specs = (P(EP, "tp"), P(EP, "tp"), P(EP, None, "tp"))
    return jax.shard_map(per_device, mesh=torus, in_specs=in_specs, out_specs=out_specs, check_vma=False)
```

time: 290 us -> 91.6 us (0.32)
  waiting for transfers between devices: 139 us -> 0 us
  Pallas kernels: 0 us -> 86.3 us
  blocking collectives: 77.3 us -> 0 us
  local copies, waits for them, and re-layouts: 27.9 us -> 4.39 us
  between operations: 15 us -> 0.65 us
  matrix products: 13.1 us -> 0 us
  starting transfers between devices: 9.9 us -> 0 us
  other arithmetic: 6.64 us -> 0 us
    all_gather x2 -> x0, waiting for transfers between devices: 120 us -> none  [the longest x1 94.4 us: gather_turned(): lax.all_gather(both, axis, axis=0, tiled=True)]
    pallas_call x0 -> x1, Pallas kernels: none -> 86.3 us  [per_device(): pl.pallas_call(kernel, name='layer', out_shape=(jax.ShapeDtypeStruct((S,...]
    all_to_all x5 -> x0, blocking collectives: 48.1 us -> none  [the longest x1 31.3 us: per_device(): lax.all_to_all(outgoing, EP, split_axis=0, concat_axis=0, tiled=True)]
    all_gather x2 -> x0, blocking collectives: 26.8 us -> none  [gathered_by_axis(): x = lax.all_gather(x, axis, axis=dim, tiled=True)]
    all_to_all x2 -> x0, waiting for transfers between devices: 19.8 us -> none  [the longest x1 19.8 us: per_device(): lax.all_to_all(partial_value.astype(jnp.bfloat16), EP, split_axis=0, conc...]
    dot_general x8 -> x0, matrix products: 13.1 us -> none  [the longest x1 4.26 us: per_device(): jnp.einsum('nd,dsc->nsc', scaled, jnp.stack(gather_turned((input_weight,...]
    unnamed x31 -> x3, local copies, waits for them, and re-layouts: 15.6 us -> 4.39 us
    all_to_all x2 -> x0, starting transfers between devices: 9.82 us -> none  [the longest x1 6.62 us: per_device(): lax.all_to_all(partial_value.astype(jnp.bfloat16), EP, split_axis=0, conc...]
  transfers between devices with their start and end apart: 4 -> 0, of which waited for: 3 -> 0; matrix products, arithmetic and copies ran while one was open for 10% -> 0% of each run, Pallas kernels for 0% -> 0%
where the time goes in v1:
time: 91.6 us; the launch traced here: 91.3 us
  Pallas kernels  86.3 us (94%)
  local copies, waits for them, and re-layouts  4.39 us (5%)
    pallas_call x1, Pallas kernels, per_device(): pl.pallas_call(kernel, name='layer', out_shape=(jax.ShapeDtypeStruct((S,...  86.3 us
    unnamed x3, local copies, waits for them, and re-layouts  4.39 us

profile of v1, /device:TPU:2, one launch (start us, length us, event | category | flops | bytes accessed | tf_op | source)
XLA Modules:
  0.0 91.3 jit_solution(13062079184988028862)
XLA Ops:
  0.6 86.3 %layer.1 = (bf16[16,1024]{1,0:T(8,128)(2,1)}, f32[16,1024]{1,0:T(8,128)}, bf16[3,16,1024]{2,1,0:T(8,128)(2,1)}) custom-call(bf16[16,1024]{1,0:T(8,128)(2,1)} %refs_0_.1, f32[16,1024]{1,0:T(8,128)} %refs_1_.1, bf16[3,16,1024]{2,1,0:T(8,128)(2,1)} %bitcast.19, f32[1,1024]{1,0:T(1,128)} %bitcast.23, bf16[16,1024]{1,0:T(8,128)(2,1)} %bitcast.20, ...), custom_call_target="tpu_custom_call" | custom-call | tf_op jit(solution)/shard_map/layer/pallas_call | solution.py:403
  86.9 1.4 %copy.23 = bf16[16,1024]{1,0:T(8,128)(2,1)} copy(bf16[16,1024]{1,0:T(8,128)(2,1)} %get-tuple-element.12) | data formatting | bytes 65536
  88.3 1.5 %copy.24 = f32[16,1024]{1,0:T(8,128)} copy(f32[16,1024]{1,0:T(8,128)} %get-tuple-element.13) | data formatting | bytes 131072
  89.7 1.5 %copy.25 = bf16[16,3,1024]{2,0,1:T(8,128)(2,1)} copy(bf16[16,3,1024]{2,0,1:T(8,128)(2,1)} %bitcast.18) | data formatting | bytes 196608

commit v2 on v1

--- a/solution.py
+++ b/solution.py
@@ -11,6 +11,8 @@
 MESH = pl.DeviceIdType.MESH
 NZ, NY, NX = 8, 4, 4
 ORDER = {8: (1, 7, 2, 6, 3, 5, 4), 4: (1, 3, 2)}
+ZORD, XORD = (0,) + ORDER[8], (0,) + ORDER[4]
+GROUPS = ((0, 5), (5, 3))
 BF, F32 = jnp.bfloat16, jnp.float32
 EPSILON = 1e-6
 DECAY_POWER = 8.0
@@ -38,16 +40,18 @@
         wu=vm((Q, 2, LANES, FD), BF),
         wd=vm((FD, D), BF),
         xs=vm((NZ, S, H), BF),
-        ms=vm((NZ, S, H), BF),
-        wt=vm((3, 4, 4, S, H), BF),
+        ms=vm((NY, S, H), BF),
+        wt=vm((2, 4, 4, S, H), BF),
+        wo=vm((NX, NZ, S, H), BF),
         ps=vm((NZ * S, 512), BF),
         pr=vm((NZ * S, 512), BF),
         ss=vm((NZ, S, 512), BF),
         ra=vm((4, S, 512), BF),
-        ps2=vm((NZ * S, 256), BF),
-        pr2=vm((NZ * S, 256), BF),
-        ss2=vm((NZ, S, 256), BF),
-        rb=vm((4, S, 256), BF),
+        po=vm((2, NY * S, 256), F32),
+        ps2=vm((2, NY * S, 256), BF),
+        pr2=vm((NY * S, 256), BF),
+        ss2=vm((NY, S, 256), BF),
+        rb=vm((NY, S, 256), BF),
         qs=vm((2, S, LANES), F32),
         qr=vm((2, S, LANES), F32),
         bd=vm((2, 4, 256, 256), BF),
@@ -61,8 +65,9 @@
         hs=vm((NX, 64, H), BF),
         hr=vm((NX, 64, H), BF),
         own=vm((NX, 64, H), F32),
-        xsend=vm((NX, 64, H), BF),
-        xrecv=vm((NX, 64, H), BF),
+        xsend=vm((NX, 2, 32, H), BF),
+        rl=vm((2, 32, H), BF),
+        xrecv=vm((2, 2, 32, H), BF),
         ysend=vm((NY, NZ, 16, LANES), BF),
         ry=vm((NY, NZ, 16, LANES), BF),
         rz=vm((NZ, NY, 16, LANES), BF),
@@ -73,19 +78,22 @@
         stores=dma((3,)),
         x_s=dma((8,)), x_r=dma((8,)),
         m_s=dma((8,)), m_r=dma((8,)),
-        w1_s=dma((2, 4)), w1_r=dma((2, 4)),
-        w2_s=dma((2, 4)), w2_r=dma((2, 4)),
+        w_s=dma((16,)), w_r=dma((16,)),
+        oz_s=dma((8,)), oz_r=dma((8,)),
+        ox_s=dma((4,)), ox_r=dma((4,)),
         t_s=dma((4,)), t_r=dma((4,)),
         a_s=dma((8,)), a_r=dma((4,)),
-        b_s=dma((8,)), b_r=dma((4,)),
+        b_s=dma((4,)), b_r=dma((4,)),
         dz_s=dma((8,)), dz_r=dma((8,)),
-        dy_s=dma((4,)), dy_r=dma((4,)),
-        dx_s=dma((4,)), dx_r=dma((4,)),
-        dt_s=dma((4,)), dt_r=dma((4,)),
+        dy_s=dma((2, 4)), dy_r=dma((2, 4)),
+        dx_s=dma((2, 4, 2)), dx_r=dma((2, 4, 2)),
+        dl_s=dma((2, 4)), dl_r=dma((2, 4)),
+        dt_s=dma((4, 2)), dt_r=dma((4, 2)),
         ht_s=dma((4,)), ht_r=dma((4,)),
-        rx_s=dma((4,)), rx_r=dma((4,)),
+        rl_s=dma((2,)), rl_r=dma((2,)),
+        rx_s=dma((2, 2)), rx_r=dma((2, 2)),
         ry_s=dma((4,)), ry_r=dma((4,)),
-        rz_s=dma((8,)), rz_r=dma((8,)),
+        rz_s=dma((2, 8)), rz_r=dma((2, 8)),
     )
 
 
@@ -132,7 +140,7 @@
     b = x + tp * (y - x)
     plan = [
         (stream, k["sv"]), (gain1, k["g1v"]),
-        (w_in, k["wt"].at[0, a, b]), (w_br, k["wt"].at[1, a, b]), (w_out, k["wt"].at[2, a, b]),
+        (w_in, k["wt"].at[0, a, b]), (w_br, k["wt"].at[1, a, b]), (w_out, k["wo"].at[x, z]),
         (rg, k["rgv"]), (ig, k["igv"]), (routes, k["rtv"]), (rw, k["rwv"]),
         (conv, k["cv"]), (taps, k["tv"]), (decay, k["dv"]), (hidden, k["hv"]), (gain2, k["g2v"]),
         (eg.at[0], k["wg"].at[:, 0]), (eg.at[1], k["wg"].at[:, 1]),
@@ -159,31 +167,56 @@
         loads[i].wait()
     pl.semaphore_wait(barrier, 14)
 
-    for kinds, n in ((pl.ds(0, 2), 0), (pl.ds(2, 1), 1)):
-        for d in ORDER[4]:
-            there = {"y": lax.rem(y + d * tp, NY), "x": lax.rem(x + d * other, NX)}
-            block = k["wt"].at[kinds, a, b]
-            start(block, block, k["w1_s"].at[n, d], k["w1_r"].at[n, d], there)
-        if n == 0:
-            for d in ORDER[8]:
-                start(k["xs"].at[z], k["xs"].at[z], k["x_s"].at[d], k["x_r"].at[d], {"z": lax.rem(z + d, NZ)})
-            start(k["qs"].at[0], k["qr"].at[0], k["t_s"].at[0], k["t_r"].at[0], {"tp": other})
-
-    def second_stage(kinds, n):
-        for d in ORDER[4]:
-            block = k["wt"].at[kinds, a, lax.rem(b - d + 4, 4)]
-            await_recv(block, k["w1_s"].at[n, d], k["w1_r"].at[n, d], {"tp": other})
-        for d in ORDER[4]:
-            there = {"y": lax.rem(y + d * other, NY), "x": lax.rem(x + d * tp, NX)}
-            block = k["wt"].at[kinds, a]
-            start(block, block, k["w2_s"].at[n, d], k["w2_r"].at[n, d], there)
-
-    def second_arrived(kinds, n):
-        for d in ORDER[4]:
-            block = k["wt"].at[kinds, lax.rem(a - d + 4, 4)]
-            await_recv(block, k["w2_s"].at[n, d], k["w2_r"].at[n, d], {"tp": other})
-
-    second_stage(pl.ds(0, 2), 0)
+    def along_b(d):
+        return {"y": lax.rem(y + d * tp, NY), "x": lax.rem(x + d * other, NX)}
+
+    def along_a(d):
+        return {"y": lax.rem(y + d * other, NY), "x": lax.rem(x + d * tp, NX)}
+
+    both = pl.ds(0, 2)
+
+    def block(da, db, kinds=both):
+        return k["wt"].at[kinds, lax.rem(a - da + 4, 4), lax.rem(b - db + 4, 4)]
+
+    def push(ref, i, where):
+        start(ref, ref, k["w_s"].at[i], k["w_r"].at[i], where)
+
+    def pull(ref, i):
+        await_recv(ref, k["w_s"].at[i], k["w_r"].at[i], {"tp": other})
+
+    def push_a(i):
+        push(block(0, XORD[i]), 4 + 2 * i, along_a(1))
+        push(block(0, XORD[i]), 5 + 2 * i, along_a(3))
+
+    push(block(0, 0), 0, along_b(1))
+    push(block(0, 0), 1, along_b(3))
+    push_a(0)
+    for d in ORDER[8]:
+        start(k["xs"].at[z], k["xs"].at[z], k["x_s"].at[d], k["x_r"].at[d], {"z": lax.rem(z + d, NZ)})
+    start(k["qs"].at[0], k["qr"].at[0], k["t_s"].at[0], k["t_r"].at[0], {"tp": other})
+    for d in ORDER[8]:
+        mine = k["wo"].at[x, z]
+        start(mine, mine, k["oz_s"].at[d], k["oz_r"].at[d], {"z": lax.rem(z + d, NZ)})
+    first, second = pl.ds(0, 1), pl.ds(1, 1)
+    with jax.named_scope("w_b"):
+        pull(block(0, 1), 0)
+        push(block(0, 1, first), 2, along_b(1))
+        push_a(1)
+        pull(block(0, 3), 1)
+        push(block(0, 3, second), 3, along_b(3))
+        push_a(2)
+    with jax.named_scope("w_a0"):
+        pull(block(1, 0), 4)
+        push(block(1, 0), 12, along_a(1))
+    with jax.named_scope("w_b2"):
+        pull(block(0, 2, first), 2)
+        pull(block(0, 2, second), 3)
+        push_a(3)
+    with jax.named_scope("w_a1"):
+        pull(block(1, 1), 6)
+        push(block(1, 1), 13, along_a(1))
+        pull(block(3, 3), 9)
+        push(block(3, 3), 14, along_a(3))
 
     loads[5].wait()
     loads[6].wait()
@@ -205,14 +238,38 @@
     before = (iota(square, 0) < iota(square, 1) % S).astype(BF)
     rank = dot(hits.astype(BF), before)
     slot = (iota(rows, 0) // Q % CAP).astype(F32)
-    chosen = (hits > 0.5) & (rank == slot) & (iota(rows, 0) % Q == iota(rows, 1) // S)
+    same = iota(rows, 0) % Q == iota(rows, 1) // S
+    chosen = (hits > 0.5) & (rank == slot) & same
     k["pm"][...] = jnp.where(chosen, 1.0, 0.0).astype(BF)
+    step = iota(rows, 0) // 16 % 4
+    step = jnp.where(step == 2, 3, jnp.where(step == 3, 2, step))
+    expert = (iota(rows, 0) // 64 * 4 + (y + step) % 4).astype(F32)
+    hit0, hit1 = named[0:1] == expert, named[1:2] == expert
+    hits = jnp.where(hit0 | hit1, 1.0, 0.0)
+    chosen = (hits > 0.5) & (dot(hits.astype(BF), before) == slot) & same
     k["pw"][...] = jnp.where(chosen, jnp.where(hit0, weights[0:1], weights[1:2]), 0.0)
 
-    second_stage(pl.ds(2, 1), 1)
-    for d in ORDER[8]:
-        await_recv(k["xs"].at[lax.rem(z - d + NZ, NZ)], k["x_s"].at[d], k["x_r"].at[d], {"tp": other})
-    second_arrived(pl.ds(0, 2), 0)
+    with jax.named_scope("w_a2"):
+        pull(block(3, 2), 11)
+        push(block(3, 2), 15, along_a(3))
+    with jax.named_scope("w_xg"):
+        for d in ORDER[8]:
+            await_recv(k["xs"].at[lax.rem(z - d + NZ, NZ)], k["x_s"].at[d], k["x_r"].at[d], {"tp": other})
+    with jax.named_scope("w_oz"):
+        for d in ORDER[8]:
+            await_recv(k["wo"].at[x, lax.rem(z - d + NZ, NZ)], k["oz_s"].at[d], k["oz_r"].at[d], {"tp": other})
+        for i in range(2):
+            there = lax.rem(x + (1, 3)[i], NX)
+            start(k["wo"].at[x], k["wo"].at[x], k["ox_s"].at[i], k["ox_r"].at[i], {"x": there})
+    with jax.named_scope("w_aend"):
+        pull(block(3, 0), 5)
+        pull(block(3, 1), 7)
+        pull(block(1, 3), 8)
+        pull(block(1, 2), 10)
+        pull(block(2, 0), 12)
+        pull(block(2, 1), 13)
+        pull(block(2, 3), 14)
+        pull(block(2, 2), 15)
 
     def columns(kind):
         blocks = []
@@ -255,6 +312,13 @@
                 remote(k[ss].at[0], k[land].at[0], k[sends].at[d], k[lands].at[0], {"tp": other}).wait_send()
 
     project("xs", (0, 1), 512, "ps", "pr", "ss", "ra", 1, "a_s", "a_r")
+    with jax.named_scope("w_ox"):
+        half = (pl.ds(0, 4), pl.ds(4, 4))
+        for i in range(2):
+            source = k["wo"].at[lax.rem(x + (3, 1)[i], NX)]
+            await_recv(source, k["ox_s"].at[i], k["ox_r"].at[i], {"tp": other})
+            passed = source.at[half[i]]
+            start(passed, passed, k["ox_s"].at[2 + i], k["ox_r"].at[2 + i], {"x": lax.rem(x + (1, 3)[i], NX)})
     await_recv(k["qr"].at[0], k["t_s"].at[0], k["t_r"].at[0], {"tp": other})
     row_scale = lax.rsqrt((k["qs"][0] + k["qr"][0])[:, 0:1] / D + EPSILON)
     forward = (jnp.concatenate([k["ra"][i, :, 0:256] for i in range(4)], axis=1).astype(F32) * row_scale).astype(BF)
@@ -284,14 +348,36 @@
     k["nh"][...] = new_hidden
     store_hidden = pltpu.make_async_copy(k["nh"], o_hidden, k["stores"].at[1])
     store_hidden.start()
-    k["ms"][z] = (jax.nn.gelu(branch.astype(F32)) * new_hidden).astype(BF)
-    for d in ORDER[8]:
-        start(k["ms"].at[z], k["ms"].at[z], k["m_s"].at[d], k["m_r"].at[d], {"z": lax.rem(z + d, NZ)})
-    second_arrived(pl.ds(2, 1), 1)
-    for d in ORDER[8]:
-        await_recv(k["ms"].at[lax.rem(z - d + NZ, NZ)], k["m_s"].at[d], k["m_r"].at[d], {"tp": other})
-    project("ms", (2,), 256, "ps2", "pr2", "ss2", "rb", 2, "b_s", "b_r")
-    out_terms = jnp.concatenate([k["rb"][i] for i in range(4)], axis=1).astype(F32)
+    k["ms"][y] = (jax.nn.gelu(branch.astype(F32)) * new_hidden).astype(BF)
+    for d in ORDER[4]:
+        start(k["ms"].at[y], k["ms"].at[y], k["m_s"].at[d], k["m_r"].at[d], {"y": lax.rem(y + d, NY)})
+    with jax.named_scope("w_ox2"):
+        for i in range(2):
+            passed = k["wo"].at[lax.rem(x + 2, NX), half[i]]
+            await_recv(passed, k["ox_s"].at[2 + i], k["ox_r"].at[2 + i], {"tp": other})
+    with jax.named_scope("w_mg"):
+        for d in ORDER[4]:
+            await_recv(k["ms"].at[lax.rem(y - d + NY, NY)], k["m_s"].at[d], k["m_r"].at[d], {"tp": other})
+    lhs = k["ms"][...].reshape(NY * S, H)
+    for h in range(2):
+        out_columns = jnp.concatenate([k["wo"][j, 4 * h + i] for i in range(4) for j in range(NX)], axis=0)
+        part = dot(lhs, out_columns, ((1,), (1,)))
+        k["po"][h] = part
+        k["ps2"][h] = part.astype(BF)
+    start(k["ps2"].at[other], k["pr2"], k["t_s"].at[2], k["t_r"].at[2], {"tp": other})
+    with jax.named_scope("w_pt"):
+        await_recv(k["pr2"], k["t_s"].at[2], k["t_r"].at[2], {"tp": other})
+    k["ss2"][...] = (k["po"][tp] + k["pr2"][...].astype(F32)).astype(BF).reshape(NY, S, 256)
+    for d in ORDER[4]:
+        there = lax.rem(y + d, NY)
+        start(k["ss2"].at[there], k["rb"].at[y], k["b_s"].at[d], k["b_r"].at[d], {"y": there})
+    k["rb"][y] = k["ss2"][y]
+    with jax.named_scope("w_rb"):
+        for d in ORDER[4]:
+            await_recv(k["rb"].at[lax.rem(y - d + NY, NY)], k["b_s"].at[d], k["b_r"].at[d], {"tp": other})
+    out_terms = jnp.concatenate(
+        [k["rb"][j, :, i * 64 : i * 64 + 64].astype(F32) for i in range(4) for j in range(NY)], axis=1
+    )
     middle = (values + out_terms).astype(BF)
     mid_values = middle.astype(F32)
     k["qs"][1] = jnp.broadcast_to(jnp.sum(mid_values * mid_values, axis=1, keepdims=True), (S, LANES))
@@ -302,82 +388,168 @@
 
     stacked = jnp.concatenate([normed[:, q * LANES : (q + 1) * LANES] for q in range(Q)], axis=0)
     k["zsend"][...] = dot(k["pm"][...], stacked).astype(BF).reshape(NZ, NY, 16, LANES)
-    for d in ORDER[8]:
-        there = lax.rem(z + d, NZ)
-        start(k["zsend"].at[there], k["zrecv"].at[z], k["dz_s"].at[d], k["dz_r"].at[d], {"z": there})
-    k["zrecv"][z] = k["zsend"][z]
-    for d in ORDER[8]:
-        await_recv(k["zrecv"].at[lax.rem(z - d + NZ, NZ)], k["dz_s"].at[d], k["dz_r"].at[d], {"tp": other})
-    for d in ORDER[4]:
-        there = lax.rem(y + d, NY)
-        start(k["zrecv"].at[:, there], k["fb"].at[tp, x, y], k["dy_s"].at[d], k["dy_r"].at[d], {"y": there})
-    k["fb"][tp, x, y] = k["zrecv"][:, y]
-    for d in ORDER[4]:
-        block = k["fb"].at[tp, x, lax.rem(y - d + NY, NY)]
-        await_recv(block, k["dy_s"].at[d], k["dy_r"].at[d], {"tp": other})
-    for d in ORDER[4]:
-        there = lax.rem(x + d, NX)
-        start(k["fb"].at[tp, x], k["fb"].at[tp, x], k["dx_s"].at[d], k["dx_r"].at[d], {"x": there})
-    for d in (0,) + ORDER[4]:
-        block = k["fb"].at[tp, lax.rem(x - d + NX, NX)]
-        if d:
-            await_recv(block, k["dx_s"].at[d], k["dx_r"].at[d], {"tp": other})
-        start(block, block, k["dt_s"].at[d], k["dt_r"].at[d], {"tp": other})
-    for i in range(14, 19):
-        loads[i].wait()
-    for d in (0,) + ORDER[4]:
-        block = k["fb"].at[other, lax.rem(x - d + NX, NX)]
-        await_recv(block, k["dt_s"].at[d], k["dt_r"].at[d], {"tp": other})
+    for i in range(1, 8):
+        there = lax.rem(z + ZORD[i], NZ)
+        start(k["zsend"].at[there], k["zrecv"].at[i], k["dz_s"].at[i], k["dz_r"].at[i], {"z": there})
+    k["zrecv"][0] = k["zsend"][z]
+    steps = (1, 3)
+
+    def part_of(xi, yi, g, h=tp):
+        return k["fb"].at[h, xi, yi, pl.ds(*GROUPS[g])]
+
+    def send_x(yi, g):
+        for n in range(2):
+            where = {"x": lax.rem(x + steps[n], NX)}
+            start(part_of(0, yi, g), part_of(1 + n, yi, g), k["dx_s"].at[n, yi, g], k["dx_r"].at[n, yi, g], where)
+
+    def wait_x(n, yi, g):
+        await_recv(part_of(1 + n, yi, g), k["dx_s"].at[n, yi, g], k["dx_r"].at[n, yi, g], {"tp": other})
+        if yi // 2 == n:
+            where = {"x": lax.rem(x + steps[n], NX)}
+            start(part_of(1 + n, yi, g), part_of(3, yi, g), k["dl_s"].at[g, yi], k["dl_r"].at[g, yi], where)
+
+    def send_core(xi, g):
+        ref = k["fb"].at[tp, xi, :, pl.ds(*GROUPS[g])]
+        start(ref, ref, k["dt_s"].at[xi, g], k["dt_r"].at[xi, g], {"tp": other})
+
+    for g, (low, count) in enumerate(GROUPS):
+        with jax.named_scope(f"w_dz{g}"):
+            for i in range(max(low, 1), low + count):
+                await_recv(k["zrecv"].at[i], k["dz_s"].at[i], k["dz_r"].at[i], {"tp": other})
+        for i in range(1, 4):
+            there = lax.rem(y + XORD[i], NY)
+            src = k["zrecv"].at[pl.ds(low, count), there]
+            start(src, part_of(0, i, g), k["dy_s"].at[g, i], k["dy_r"].at[g, i], {"y": there})
+        k["fb"][tp, 0, 0, low : low + count] = k["zrecv"][low : low + count, y]
+        send_x(0, g)
+    for g in range(2):
+        with jax.named_scope(f"w_dy{g}"):
+            for i in range(1, 4):
+                await_recv(part_of(0, i, g), k["dy_s"].at[g, i], k["dy_r"].at[g, i], {"tp": other})
+                send_x(i, g)
+        send_core(0, g)
+        with jax.named_scope(f"w_dx0{g}"):
+            wait_x(0, 0, g)
+    with jax.named_scope("w_dxr"):
+        for g in range(2):
+            wait_x(0, 1, g)
+            wait_x(1, 2, g)
+            wait_x(1, 3, g)
+    with jax.named_scope("w_dxe"):
+        for g in range(2):
+            wait_x(0, 2, g)
+            wait_x(0, 3, g)
+            send_core(1, g)
+            wait_x(1, 0, g)
+            wait_x(1, 1, g)
+            send_core(2, g)
+    with jax.named_scope("w_dxl"):
+        for g in range(2):
+            for yi in range(4):
+                await_recv(part_of(3, yi, g), k["dl_s"].at[g, yi], k["dl_r"].at[g, yi], {"tp": other})
+            send_core(3, g)
+    with jax.named_scope("w_we"):
+        for i in range(14, 19):
+            loads[i].wait()
 
     turn = iota(square, 1) == iota(square, 0) % 16 * Q + iota(square, 0) // 16
     turn = jnp.where(turn, 1.0, 0.0).astype(BF)
-    for g in range(NX * NY):
-        pair = jnp.concatenate([k["fb"][h, g // NY, g % NY].reshape(LANES, LANES) for h in range(2)], axis=1)
-        turned = dot(turn, pair).astype(BF)
-        for q in range(Q):
-            k["ab"][g * 16 : g * 16 + 16, q * 256 : q * 256 + 256] = turned[q * 16 : q * 16 + 16]
+    for xi in range(NX):
+        with jax.named_scope(f"w_dt{xi}"):
+            for g in range(2):
+                ref = k["fb"].at[other, xi, :, pl.ds(*GROUPS[g])]
+                await_recv(ref, k["dt_s"].at[xi, g], k["dt_r"].at[xi, g], {"tp": other})
+        for yi in range(NY):
+            pair = jnp.concatenate([k["fb"][h, xi, yi].reshape(LANES, LANES) for h in range(2)], axis=1)
+            turned = dot(turn, pair).astype(BF)
+            at = (xi * NY + yi) * 16
+            for q in range(Q):
+                k["ab"][at : at + 16, q * 256 : q * 256 + 256] = turned[q * 16 : q * 16 + 16]
     gate_act = dot(k["ab"][...], k["wg"][...].reshape(D, FD))
     upper = dot(k["ab"][...], k["wu"][...].reshape(D, FD))
     k["ib"][...] = (jax.nn.silu(gate_act) * upper).astype(BF)
 
-    for d in ORDER[4] + (0,):
-        there = lax.rem(x + d, NX)
-        inner = k["ib"][pl.ds(pl.multiple_of(there * 64, 64), 64)]
-        theirs = pl.ds(pl.multiple_of(other * H, H), H)
-        ours = pl.ds(pl.multiple_of(tp * H, H), H)
-        k["hs"][there] = dot(inner, k["wd"][:, theirs]).astype(BF)
-        start(k["hs"].at[there], k["hr"].at[there], k["ht_s"].at[d], k["ht_r"].at[d], {"tp": other})
-        k["own"][there] = dot(inner, k["wd"][:, ours])
-    for d in ORDER[4] + (0,):
-        there = lax.rem(x + d, NX)
-        await_recv(k["hr"].at[there], k["ht_s"].at[d], k["ht_r"].at[d], {"tp": other})
-        whole = k["own"][there] + k["hr"][there].astype(F32)
-        if d:
-            k["xsend"][there] = whole.astype(BF)
-            start(k["xsend"].at[there], k["xrecv"].at[x], k["rx_s"].at[d], k["rx_r"].at[d], {"x": there})
-    for d in ORDER[4]:
-        source = lax.rem(x - d + NX, NX)
-        await_recv(k["xrecv"].at[source], k["rx_s"].at[d], k["rx_r"].at[d], {"tp": other})
-        whole = whole + k["xrecv"][source].astype(F32)
-    whole = whole.astype(BF)
+    theirs = pl.ds(pl.multiple_of(other * H, H), H)
+    ours = pl.ds(pl.multiple_of(tp * H, H), H)
+    ahead, behind = {"x": lax.rem(x + 1, NX)}, {"x": lax.rem(x + 3, NX)}
+
+    def down(xi):
+        inner = k["ib"][xi * 64 : xi * 64 + 64]
+        k["hs"][xi] = dot(inner, k["wd"][:, theirs]).astype(BF)
+        start(k["hs"].at[xi], k["hr"].at[xi], k["ht_s"].at[xi], k["ht_r"].at[xi], {"tp": other})
+        k["own"][xi] = dot(inner, k["wd"][:, ours])
+
+    def whole(xi):
+        with jax.named_scope(f"w_ht{xi}"):
+            await_recv(k["hr"].at[xi], k["ht_s"].at[xi], k["ht_r"].at[xi], {"tp": other})
+        return k["own"][xi] + k["hr"][xi].astype(F32)
+
+    def send_sum(xi, half, rows):
+        n = 2 - xi
+        k["xsend"][xi, half] = rows.astype(BF)
+        start(
+            k["xsend"].at[xi, half],
+            k["xrecv"].at[n, half],
+            k["rx_s"].at[n, half],
+            k["rx_r"].at[n, half],
+            (ahead, behind)[n],
+        )
+
+    down(3)
+    down(2)
+    far = whole(3)
+    for half in range(2):
+        k["xsend"][3, half] = far[half * 32 : half * 32 + 32].astype(BF)
+        src, dst = k["xsend"].at[3, half], k["rl"].at[half]
+        start(src, dst, k["rl_s"].at[half], k["rl_r"].at[half], (ahead, behind)[half])
+    down(1)
+    next_sum = whole(2)
+    send_sum(2, 1, next_sum[32:])
+    down(0)
+    last_sum = whole(1)
+    send_sum(1, 0, last_sum[:32])
+    with jax.named_scope("w_rl0"):
+        await_recv(k["rl"].at[0], k["rl_s"].at[0], k["rl_r"].at[0], {"tp": other})
+    send_sum(2, 0, next_sum[:32] + k["rl"][0].astype(F32))
+    with jax.named_scope("w_rl1"):
+        await_recv(k["rl"].at[1], k["rl_s"].at[1], k["rl_r"].at[1], {"tp": other})
+    send_sum(1, 1, last_sum[32:] + k["rl"][1].astype(F32))
+    home = whole(0)
     back = iota(square, 0) == iota(square, 1) % 16 * Q + iota(square, 1) // 16
     back = jnp.where(back, 1.0, 0.0).astype(BF)
-    for g in range(NY):
-        part = whole[g * 16 : g * 16 + 16]
-        part = jnp.concatenate([part[:, q * LANES : (q + 1) * LANES] for q in range(Q)], axis=0)
-        k["ysend"][g] = dot(back, part).astype(BF).reshape(NZ, 16, LANES)
-    for d in ORDER[4]:
-        there = lax.rem(y + d, NY)
-        start(k["ysend"].at[there], k["ry"].at[y], k["ry_s"].at[d], k["ry_r"].at[d], {"y": there})
-    k["ry"][y] = k["ysend"][y]
-    for d in ORDER[4]:
-        await_recv(k["ry"].at[lax.rem(y - d + NY, NY)], k["ry_s"].at[d], k["ry_r"].at[d], {"tp": other})
-    for d in ORDER[8]:
-        there = lax.rem(z + d, NZ)
-        start(k["ry"].at[:, there], k["rz"].at[z], k["rz_s"].at[d], k["rz_r"].at[d], {"z": there})
-    k["rz"][z] = k["ry"][:, z]
-    for d in ORDER[8]:
-        await_recv(k["rz"].at[lax.rem(z - d + NZ, NZ)], k["rz_s"].at[d], k["rz_r"].at[d], {"tp": other})
+    for half in (1, 0):
+        with jax.named_scope(f"w_rx{half}"):
+            for n in range(2):
+                await_recv(k["xrecv"].at[n, half], k["rx_s"].at[n, half], k["rx_r"].at[n, half], {"tp": other})
+        rows = home[half * 32 : half * 32 + 32]
+        rows = (rows + k["xrecv"][0, half].astype(F32) + k["xrecv"][1, half].astype(F32)).astype(BF)
+        for yi in (3, 2) if half else (1, 0):
+            part = rows[yi % 2 * 16 : yi % 2 * 16 + 16]
+            part = jnp.concatenate([part[:, q * LANES : (q + 1) * LANES] for q in range(Q)], axis=0)
+            part = dot(back, part).astype(BF).reshape(NZ, 16, LANES)
+            if yi:
+                k["ysend"][yi] = part
+                where = {"y": lax.rem(y - XORD[yi] + NY, NY)}
+                start(k["ysend"].at[yi], k["ry"].at[yi], k["ry_s"].at[yi], k["ry_r"].at[yi], where)
+            else:
+                k["ry"][0] = part
+    for half in (1, 0):
+        with jax.named_scope(f"w_ry{half}"):
+            for yi in (2, 3) if half else (1,):
+                await_recv(k["ry"].at[yi], k["ry_s"].at[yi], k["ry_r"].at[yi], {"tp": other})
+        pair = pl.ds(2 * half, 2)
+        for i in range(1, 8):
+            there = lax.rem(z - ZORD[i] + NZ, NZ)
+            start(
+                k["ry"].at[pair, i], k["rz"].at[z, pair], k["rz_s"].at[half, i], k["rz_r"].at[half, i], {"z": there}
+            )
+        k["rz"][z, 2 * half : 2 * half + 2] = k["ry"][2 * half : 2 * half + 2, 0]
+    with jax.named_scope("w_rz"):
+        for half in (1, 0):
+            pair = pl.ds(2 * half, 2)
+            for i in range(1, 8):
+                ref = k["rz"].at[lax.rem(z + ZORD[i], NZ), pair]
+                await_recv(ref, k["rz_s"].at[half, i], k["rz_r"].at[half, i], {"tp": other})
     returned = k["rz"][...].reshape(EXPERTS * 16, LANES).astype(F32)
     mix = dot(k["pw"][...], returned, ((0,), (0,)), HIGHEST)
     expert_mix = jnp.concatenate([mix[q * S : (q + 1) * S] for q in range(Q)], axis=1)
@@ -388,10 +560,14 @@
     for c in sent:
         c.wait_send()
     sends_done("ss", "ra", "a_s", "a_r")
-    sends_done("ss2", "rb", "b_s", "b_r")
     store_conv.wait()
     store_hidden.wait()
     store_stream.wait()
+
+
+def handed_on(*refs):
+    for src, dst in zip(refs[:3], refs[3:]):
+        dst[...] = src[...]
 
 
 def per_device(
@@ -433,7 +609,14 @@
         expert_up.reshape(2, Q, LANES, FD),
         expert_down,
     )
-    new_stream, new_hidden, new_conv = outs
+    vmem = pl.BlockSpec(memory_space=pltpu.VMEM)
+    new_stream, new_hidden, new_conv = pl.pallas_call(
+        handed_on,
+        name="handed_on",
+        out_shape=tuple(jax.ShapeDtypeStruct(o.shape, o.dtype) for o in outs),
+        in_specs=[vmem] * 3,
+        out_specs=(vmem,) * 3,
+    )(*outs)
     return new_stream, new_hidden, new_conv.transpose(1, 0, 2)
 
 

time: 91.6 us -> 84.2 us (0.919)
  local copies, waits for them, and re-layouts: 4.39 us -> 0 us
  Pallas kernels: 86.3 us -> 82.4 us
    pallas_call x1, Pallas kernels: 86.3 us -> 80.7 us  [per_device(): pl.pallas_call(kernel, name='layer', out_shape=(jax.ShapeDtypeStruct((S,...]
    unnamed x3 -> x0, local copies, waits for them, and re-layouts: 4.39 us -> none
    pallas_call x0 -> x1, Pallas kernels: none -> 1.63 us  [per_device(): pl.pallas_call(handed_on, name='handed_on', out_shape=tuple((jax.ShapeDty...]
where the time goes in v2:
time: 84.2 us; the launch traced here: 83 us
  Pallas kernels  82.4 us (98%)
    pallas_call x1, Pallas kernels, per_device(): pl.pallas_call(kernel, name='layer', out_shape=(jax.ShapeDtypeStruct((S,...  80.7 us

profile of v2, /device:TPU:2, one launch (start us, length us, event | category | flops | bytes accessed | tf_op | source)
XLA Modules:
  0.0 83.0 jit_solution(14976379567954930697)
XLA Ops:
  0.6 80.7 %layer.1 = (bf16[16,1024]{1,0:T(8,128)(2,1)}, f32[16,1024]{1,0:T(8,128)}, bf16[3,16,1024]{2,1,0:T(8,128)(2,1)}) custom-call(bf16[16,1024]{1,0:T(8,128)(2,1)} %refs_0_.1, f32[16,1024]{1,0:T(8,128)} %refs_1_.1, bf16[3,16,1024]{2,1,0:T(8,128)(2,1)} %bitcast.18, f32[1,1024]{1,0:T(1,128)} %bitcast.22, bf16[16,1024]{1,0:T(8,128)(2,1)} %bitcast.19, ...), custom_call_target="tpu_custom_call" | custom-call | tf_op jit(solution)/shard_map/layer/pallas_call | solution.py:579
  81.4 1.6 %handed_on.1 = (bf16[16,1024]{1,0:T(8,128)(2,1)}, f32[16,1024]{1,0:T(8,128)}, bf16[3,16,1024]{2,1,0:T(8,128)(2,1)}) custom-call(bf16[16,1024]{1,0:T(8,128)(2,1)} %get-tuple-element.9.refs_0_, f32[16,1024]{1,0:T(8,128)} %get-tuple-element.10.refs_1_, bf16[3,16,1024]{2,1,0:T(8,128)(2,1)} %get-tuple-element.11.refs_2_), custom_call_target="tpu_custom_call" | custom-call | tf_op jit(solution)/shard_map/handed_on/pallas_call | solution.py:613

commit v3 on v2

--- a/solution.py
+++ b/solution.py
@@ -10,8 +10,8 @@
 EP_TP = ("z", "y", "x", "tp")
 MESH = pl.DeviceIdType.MESH
 NZ, NY, NX = 8, 4, 4
-ORDER = {8: (1, 7, 2, 6, 3, 5, 4), 4: (1, 3, 2)}
-ZORD, XORD = (0,) + ORDER[8], (0,) + ORDER[4]
+ORDER = {8: (4, 3, 5, 2, 6, 1, 7), 4: (2, 1, 3)}
+ZORD, XORD = (0, 1, 7, 2, 6, 3, 5, 4), (0, 1, 3, 2)
 GROUPS = ((0, 5), (5, 3))
 BF, F32 = jnp.bfloat16, jnp.float32
 EPSILON = 1e-6
@@ -47,11 +47,8 @@
         pr=vm((NZ * S, 512), BF),
         ss=vm((NZ, S, 512), BF),
         ra=vm((4, S, 512), BF),
-        po=vm((2, NY * S, 256), F32),
-        ps2=vm((2, NY * S, 256), BF),
-        pr2=vm((NY * S, 256), BF),
-        ss2=vm((NY, S, 256), BF),
-        rb=vm((NY, S, 256), BF),
+        ps2=vm((2, NY, S, 256), BF),
+        rb=vm((2, NY, S, 256), BF),
         qs=vm((2, S, LANES), F32),
         qr=vm((2, S, LANES), F32),
         bd=vm((2, 4, 256, 256), BF),
@@ -66,32 +63,27 @@
         hr=vm((NX, 64, H), BF),
         own=vm((NX, 64, H), F32),
         xsend=vm((NX, 2, 32, H), BF),
-        rl=vm((2, 32, H), BF),
-        xrecv=vm((2, 2, 32, H), BF),
+        xrecv=vm((NX, 2, 32, H), BF),
         ysend=vm((NY, NZ, 16, LANES), BF),
         ry=vm((NY, NZ, 16, LANES), BF),
         rz=vm((NZ, NY, 16, LANES), BF),
-        nh=vm((S, H), F32),
-        nc=vm((3, S, H), BF),
-        ns=vm((S, H), BF),
         loads=dma((24,)),
-        stores=dma((3,)),
         x_s=dma((8,)), x_r=dma((8,)),
         m_s=dma((8,)), m_r=dma((8,)),
-        w_s=dma((16,)), w_r=dma((16,)),
+        w_s=dma((5, 4)), w_r=dma((5, 4)),
         oz_s=dma((8,)), oz_r=dma((8,)),
-        ox_s=dma((4,)), ox_r=dma((4,)),
+        ox_s=dma((2, 8)), ox_r=dma((2, 8)),
+        ol_s=dma((8,)), ol_r=dma((8,)),
         t_s=dma((4,)), t_r=dma((4,)),
         a_s=dma((8,)), a_r=dma((4,)),
-        b_s=dma((4,)), b_r=dma((4,)),
+        b_s=dma((2, 4)), b_r=dma((2, 4)),
         dz_s=dma((8,)), dz_r=dma((8,)),
         dy_s=dma((2, 4)), dy_r=dma((2, 4)),
-        dx_s=dma((2, 4, 2)), dx_r=dma((2, 4, 2)),
+        dx_s=dma((3, 4, 2)), dx_r=dma((3, 4, 2)),
         dl_s=dma((2, 4)), dl_r=dma((2, 4)),
         dt_s=dma((4, 2)), dt_r=dma((4, 2)),
         ht_s=dma((4,)), ht_r=dma((4,)),
-        rl_s=dma((2,)), rl_r=dma((2,)),
-        rx_s=dma((2, 2)), rx_r=dma((2, 2)),
+        rx_s=dma((4, 2)), rx_r=dma((4, 2)),
         ry_s=dma((4,)), ry_r=dma((4,)),
         rz_s=dma((2, 8)), rz_r=dma((2, 8)),
     )
@@ -134,6 +126,9 @@
         n = {"z": NZ, "y": NY, "x": NX}[axis]
         for d in ORDER[n]:
             pl.semaphore_signal(barrier, inc=1, device_id={axis: lax.rem(me + d, n)}, device_id_type=MESH)
+    for d in ORDER[4]:
+        there = {"y": lax.rem(y + d, NY), "tp": other}
+        pl.semaphore_signal(barrier, inc=1, device_id=there, device_id_type=MESH)
     pl.semaphore_signal(barrier, inc=1, device_id={"tp": other}, device_id_type=MESH)
 
     a = y + tp * (x - y)
@@ -163,61 +158,6 @@
     values = k["sv"][...].astype(F32)
     k["xs"][z] = (values * k["g1v"][...]).astype(BF)
     k["qs"][0] = jnp.broadcast_to(jnp.sum(values * values, axis=1, keepdims=True), (S, LANES))
-    for i in (2, 3, 4):
-        loads[i].wait()
-    pl.semaphore_wait(barrier, 14)
-
-    def along_b(d):
-        return {"y": lax.rem(y + d * tp, NY), "x": lax.rem(x + d * other, NX)}
-
-    def along_a(d):
-        return {"y": lax.rem(y + d * other, NY), "x": lax.rem(x + d * tp, NX)}
-
-    both = pl.ds(0, 2)
-
-    def block(da, db, kinds=both):
-        return k["wt"].at[kinds, lax.rem(a - da + 4, 4), lax.rem(b - db + 4, 4)]
-
-    def push(ref, i, where):
-        start(ref, ref, k["w_s"].at[i], k["w_r"].at[i], where)
-
-    def pull(ref, i):
-        await_recv(ref, k["w_s"].at[i], k["w_r"].at[i], {"tp": other})
-
-    def push_a(i):
-        push(block(0, XORD[i]), 4 + 2 * i, along_a(1))
-        push(block(0, XORD[i]), 5 + 2 * i, along_a(3))
-
-    push(block(0, 0), 0, along_b(1))
-    push(block(0, 0), 1, along_b(3))
-    push_a(0)
-    for d in ORDER[8]:
-        start(k["xs"].at[z], k["xs"].at[z], k["x_s"].at[d], k["x_r"].at[d], {"z": lax.rem(z + d, NZ)})
-    start(k["qs"].at[0], k["qr"].at[0], k["t_s"].at[0], k["t_r"].at[0], {"tp": other})
-    for d in ORDER[8]:
-        mine = k["wo"].at[x, z]
-        start(mine, mine, k["oz_s"].at[d], k["oz_r"].at[d], {"z": lax.rem(z + d, NZ)})
-    first, second = pl.ds(0, 1), pl.ds(1, 1)
-    with jax.named_scope("w_b"):
-        pull(block(0, 1), 0)
-        push(block(0, 1, first), 2, along_b(1))
-        push_a(1)
-        pull(block(0, 3), 1)
-        push(block(0, 3, second), 3, along_b(3))
-        push_a(2)
-    with jax.named_scope("w_a0"):
-        pull(block(1, 0), 4)
-        push(block(1, 0), 12, along_a(1))
-    with jax.named_scope("w_b2"):
-        pull(block(0, 2, first), 2)
-        pull(block(0, 2, second), 3)
-        push_a(3)
-    with jax.named_scope("w_a1"):
-        pull(block(1, 1), 6)
-        push(block(1, 1), 13, along_a(1))
-        pull(block(3, 3), 9)
-        push(block(3, 3), 14, along_a(3))
-
     loads[5].wait()
     loads[6].wait()
     eye = (iota((64, 256), 1) % 64 == iota((64, 256), 0)).astype(BF)
@@ -249,27 +189,98 @@
     chosen = (hits > 0.5) & (dot(hits.astype(BF), before) == slot) & same
     k["pw"][...] = jnp.where(chosen, jnp.where(hit0, weights[0:1], weights[1:2]), 0.0)
 
-    with jax.named_scope("w_a2"):
-        pull(block(3, 2), 11)
-        push(block(3, 2), 15, along_a(3))
+    for i in (2, 3, 4):
+        loads[i].wait()
+    with jax.named_scope("w_bar"):
+        pl.semaphore_wait(barrier, 17)
+
+    def along_b(d):
+        return {"y": lax.rem(y + d * tp, NY), "x": lax.rem(x + d * other, NX)}
+
+    def along_a(d):
+        return {"y": lax.rem(y + d * other, NY), "x": lax.rem(x + d * tp, NX)}
+
+    both = pl.ds(0, 2)
+
+    def block(da, db):
+        return k["wt"].at[both, lax.rem(a - da + 4, 4), lax.rem(b - db + 4, 4)]
+
+    def push(ref, i, along):
+        for d in ORDER[4]:
+            start(ref, ref, k["w_s"].at[i, d], k["w_r"].at[i, d], along(d))
+
+    def pull(ref, i, d):
+        await_recv(ref, k["w_s"].at[i, d], k["w_r"].at[i, d], {"tp": other})
+
+    push(block(0, 0), 4, along_b)
+    push(block(0, 0), 0, along_a)
+    near = (2, 6, 1, 7)
+    lanes = (pl.ds(0, H // 2), pl.ds(H // 2, H // 2))
+
+    def along_z(d):
+        return {"z": lax.rem(z + d, NZ)}
+
+    def slot(ref, d):
+        return ref.at[lax.rem(z - d + NZ, NZ)]
+
+    def column_send(ref, ssem, rsem):
+        for d in near:
+            start(ref.at[z], ref.at[z], ssem.at[d], rsem.at[d], along_z(d))
+
+    def column_relay(ref, ssem, rsem):
+        for n, d in enumerate((2, 6)):
+            got, piece = slot(ref, d), slot(ref, d).at[:, lanes[n]]
+            await_recv(got, ssem.at[d], rsem.at[d], {"tp": other})
+            start(piece, piece, ssem.at[(0, 4)[n]], rsem.at[(0, 4)[n]], along_z(d))
+            start(got, got, ssem.at[(3, 5)[n]], rsem.at[(3, 5)[n]], along_z((1, 7)[n]))
+
+    def column_end(ref, ssem, rsem):
+        for d in (3, 5):
+            await_recv(slot(ref, d), ssem.at[d], rsem.at[d], {"tp": other})
+        for n in range(2):
+            await_recv(slot(ref, 4).at[:, lanes[n]], ssem.at[(0, 4)[n]], rsem.at[(0, 4)[n]], {"tp": other})
+
+    rows_column = (k["xs"], k["x_s"], k["x_r"])
+    weight_column = (k["wo"].at[x], k["oz_s"], k["oz_r"])
+    column_send(*rows_column)
+    start(k["qs"].at[0], k["qr"].at[0], k["t_s"].at[0], k["t_r"].at[0], {"tp": other})
+    column_send(*weight_column)
+    def spread_slot(d):
+        for n in range(2):
+            ref, where = k["wo"].at[x, lax.rem(z - d + NZ, NZ)], {"x": lax.rem(x + (1, 3)[n], NX)}
+            start(ref, ref, k["ox_s"].at[n, d], k["ox_r"].at[n, d], where)
+
+    def relay_slot(d):
+        for n in range(2):
+            ref = k["wo"].at[lax.rem(x + (3, 1)[n], NX), lax.rem(z - d + NZ, NZ)]
+            await_recv(ref, k["ox_s"].at[n, d], k["ox_r"].at[n, d], {"tp": other})
+            if n == (d in (3, 4, 5, 6)):
+                start(ref, ref, k["ol_s"].at[d], k["ol_r"].at[d], {"x": lax.rem(x + (1, 3)[n], NX)})
+
+    with jax.named_scope("w_b"):
+        for i in (1, 3, 2):
+            pull(block(0, i), 4, i)
+            push(block(0, i), i, along_a)
+    with jax.named_scope("w_xz"):
+        column_relay(*rows_column)
+    with jax.named_scope("w_oz"):
+        column_relay(*weight_column)
+        for d in (1, 7):
+            await_recv(slot(weight_column[0], d), k["oz_s"].at[d], k["oz_r"].at[d], {"tp": other})
+        for d in (0, 1, 7, 2, 6):
+            spread_slot(d)
     with jax.named_scope("w_xg"):
-        for d in ORDER[8]:
-            await_recv(k["xs"].at[lax.rem(z - d + NZ, NZ)], k["x_s"].at[d], k["x_r"].at[d], {"tp": other})
-    with jax.named_scope("w_oz"):
-        for d in ORDER[8]:
-            await_recv(k["wo"].at[x, lax.rem(z - d + NZ, NZ)], k["oz_s"].at[d], k["oz_r"].at[d], {"tp": other})
-        for i in range(2):
-            there = lax.rem(x + (1, 3)[i], NX)
-            start(k["wo"].at[x], k["wo"].at[x], k["ox_s"].at[i], k["ox_r"].at[i], {"x": there})
+        for d in (1, 7):
+            await_recv(slot(k["xs"], d), k["x_s"].at[d], k["x_r"].at[d], {"tp": other})
+        column_end(*rows_column)
+    with jax.named_scope("w_oze"):
+        column_end(*weight_column)
+        for d in (3, 5, 4):
+            spread_slot(d)
     with jax.named_scope("w_aend"):
-        pull(block(3, 0), 5)
-        pull(block(3, 1), 7)
-        pull(block(1, 3), 8)
-        pull(block(1, 2), 10)
-        pull(block(2, 0), 12)
-        pull(block(2, 1), 13)
-        pull(block(2, 3), 14)
-        pull(block(2, 2), 15)
+        for i in (0, 1, 3, 2):
+            for d in (1, 3, 2):
+                pull(block(d, i), i, d)
 
     def columns(kind):
         blocks = []
@@ -278,7 +289,7 @@
                 blocks.append(k["wt"][kind, i + tp * (j - i), j + tp * (i - j)])
         return jnp.concatenate(blocks, axis=0)
 
-    def project(rows_ref, kinds, width, ps, pr, ss, land, t, sends, lands):
+    def project(rows_ref, kinds, width, ps, pr, ss, land, t, sends, lands, meanwhile):
         lhs = k[rows_ref][...].reshape(NZ * S, H)
         part = jnp.concatenate([dot(lhs, columns(kind), ((1,), (1,))) for kind in kinds], axis=1)
 
@@ -300,6 +311,7 @@
                 remote(k[ss].at[there], k[land].at[mine], k[sends].at[d], k[lands].at[mine], {"z": there}).start()
             k[land][mine] = k[ss][z]
 
+        meanwhile()
         for i in range(4):
             @pl.when(4 * tp + i != z)
             def _():
@@ -311,14 +323,12 @@
             for d in ORDER[8]:
                 remote(k[ss].at[0], k[land].at[0], k[sends].at[d], k[lands].at[0], {"tp": other}).wait_send()
 
-    project("xs", (0, 1), 512, "ps", "pr", "ss", "ra", 1, "a_s", "a_r")
-    with jax.named_scope("w_ox"):
-        half = (pl.ds(0, 4), pl.ds(4, 4))
-        for i in range(2):
-            source = k["wo"].at[lax.rem(x + (3, 1)[i], NX)]
-            await_recv(source, k["ox_s"].at[i], k["ox_r"].at[i], {"tp": other})
-            passed = source.at[half[i]]
-            start(passed, passed, k["ox_s"].at[2 + i], k["ox_r"].at[2 + i], {"x": lax.rem(x + (1, 3)[i], NX)})
+    def output_weight():
+        with jax.named_scope("w_ox"):
+            for d in (0, 1, 7, 2, 6):
+                relay_slot(d)
+
+    project("xs", (0, 1), 512, "ps", "pr", "ss", "ra", 1, "a_s", "a_r", output_weight)
     await_recv(k["qr"].at[0], k["t_s"].at[0], k["t_r"].at[0], {"tp": other})
     row_scale = lax.rsqrt((k["qs"][0] + k["qr"][0])[:, 0:1] / D + EPSILON)
     forward = (jnp.concatenate([k["ra"][i, :, 0:256] for i in range(4)], axis=1).astype(F32) * row_scale).astype(BF)
@@ -326,11 +336,9 @@
     for i in range(9, 14):
         loads[i].wait()
     window = [k["cv"][0], k["cv"][1], k["cv"][2], forward]
-    k["nc"][0] = window[1]
-    k["nc"][1] = window[2]
-    k["nc"][2] = forward
-    store_conv = pltpu.make_async_copy(k["nc"], o_conv, k["stores"].at[0])
-    store_conv.start()
+    o_conv[0] = window[1]
+    o_conv[1] = window[2]
+    o_conv[2] = forward
     tap_rows = k["tv"][...].astype(F32)
     conv_out = sum(window[i].astype(F32) * tap_rows[i : i + 1] for i in range(4)).astype(BF)
 
@@ -345,16 +353,16 @@
     new_hidden = jnp.exp(log_decay) * k["hv"][...] + jnp.sqrt(-expm1(2.0 * log_decay)) * (
         inward * conv_out.astype(F32)
     )
-    k["nh"][...] = new_hidden
-    store_hidden = pltpu.make_async_copy(k["nh"], o_hidden, k["stores"].at[1])
-    store_hidden.start()
+    o_hidden[...] = new_hidden
     k["ms"][y] = (jax.nn.gelu(branch.astype(F32)) * new_hidden).astype(BF)
     for d in ORDER[4]:
         start(k["ms"].at[y], k["ms"].at[y], k["m_s"].at[d], k["m_r"].at[d], {"y": lax.rem(y + d, NY)})
     with jax.named_scope("w_ox2"):
-        for i in range(2):
-            passed = k["wo"].at[lax.rem(x + 2, NX), half[i]]
-            await_recv(passed, k["ox_s"].at[2 + i], k["ox_r"].at[2 + i], {"tp": other})
+        for d in (3, 5, 4):
+            relay_slot(d)
+        for d in range(NZ):
+            ref = k["wo"].at[lax.rem(x + 2, NX), lax.rem(z - d + NZ, NZ)]
+            await_recv(ref, k["ol_s"].at[d], k["ol_r"].at[d], {"tp": other})
     with jax.named_scope("w_mg"):
         for d in ORDER[4]:
             await_recv(k["ms"].at[lax.rem(y - d + NY, NY)], k["m_s"].at[d], k["m_r"].at[d], {"tp": other})
@@ -362,21 +370,23 @@
     for h in range(2):
         out_columns = jnp.concatenate([k["wo"][j, 4 * h + i] for i in range(4) for j in range(NX)], axis=0)
         part = dot(lhs, out_columns, ((1,), (1,)))
-        k["po"][h] = part
-        k["ps2"][h] = part.astype(BF)
-    start(k["ps2"].at[other], k["pr2"], k["t_s"].at[2], k["t_r"].at[2], {"tp": other})
-    with jax.named_scope("w_pt"):
-        await_recv(k["pr2"], k["t_s"].at[2], k["t_r"].at[2], {"tp": other})
-    k["ss2"][...] = (k["po"][tp] + k["pr2"][...].astype(F32)).astype(BF).reshape(NY, S, 256)
-    for d in ORDER[4]:
+        k["ps2"][h] = part.astype(BF).reshape(NY, S, 256)
+    for d in ORDER[4] + (0,):
         there = lax.rem(y + d, NY)
-        start(k["ss2"].at[there], k["rb"].at[y], k["b_s"].at[d], k["b_r"].at[d], {"y": there})
-    k["rb"][y] = k["ss2"][y]
+        for n, core in enumerate((tp, other)):
+            if d or n:
+                where = {"y": there, "tp": core}
+                start(k["ps2"].at[core, there], k["rb"].at[n, y], k["b_s"].at[n, d], k["b_r"].at[n, d], where)
+    k["rb"][0, y] = k["ps2"][tp, y]
     with jax.named_scope("w_rb"):
-        for d in ORDER[4]:
-            await_recv(k["rb"].at[lax.rem(y - d + NY, NY)], k["b_s"].at[d], k["b_r"].at[d], {"tp": other})
+        for d in ORDER[4] + (0,):
+            for n in range(2):
+                if d or n:
+                    ref = k["rb"].at[n, lax.rem(y - d + NY, NY)]
+                    await_recv(ref, k["b_s"].at[n, d], k["b_r"].at[n, d], {"tp": other})
+    landed = k["rb"][0].astype(F32) + k["rb"][1].astype(F32)
     out_terms = jnp.concatenate(
-        [k["rb"][j, :, i * 64 : i * 64 + 64].astype(F32) for i in range(4) for j in range(NY)], axis=1
+        [landed[j, :, i * 64 : i * 64 + 64] for i in range(4) for j in range(NY)], axis=1
     )
     middle = (values + out_terms).astype(BF)
     mid_values = middle.astype(F32)
@@ -388,24 +398,23 @@
 
     stacked = jnp.concatenate([normed[:, q * LANES : (q + 1) * LANES] for q in range(Q)], axis=0)
     k["zsend"][...] = dot(k["pm"][...], stacked).astype(BF).reshape(NZ, NY, 16, LANES)
-    for i in range(1, 8):
+    for i in range(7, 0, -1):
         there = lax.rem(z + ZORD[i], NZ)
         start(k["zsend"].at[there], k["zrecv"].at[i], k["dz_s"].at[i], k["dz_r"].at[i], {"z": there})
     k["zrecv"][0] = k["zsend"][z]
-    steps = (1, 3)
 
     def part_of(xi, yi, g, h=tp):
         return k["fb"].at[h, xi, yi, pl.ds(*GROUPS[g])]
 
     def send_x(yi, g):
-        for n in range(2):
-            where = {"x": lax.rem(x + steps[n], NX)}
+        for n in (2, 0, 1) if g else (0, 1):
+            where = {"x": lax.rem(x + (1, 3, 2)[n], NX)}
             start(part_of(0, yi, g), part_of(1 + n, yi, g), k["dx_s"].at[n, yi, g], k["dx_r"].at[n, yi, g], where)
 
     def wait_x(n, yi, g):
         await_recv(part_of(1 + n, yi, g), k["dx_s"].at[n, yi, g], k["dx_r"].at[n, yi, g], {"tp": other})
-        if yi // 2 == n:
-            where = {"x": lax.rem(x + steps[n], NX)}
+        if yi // 2 == n and not g:
+            where = {"x": lax.rem(x + (1, 3)[n], NX)}
             start(part_of(1 + n, yi, g), part_of(3, yi, g), k["dl_s"].at[g, yi], k["dl_r"].at[g, yi], where)
 
     def send_core(xi, g):
@@ -416,7 +425,7 @@
         with jax.named_scope(f"w_dz{g}"):
             for i in range(max(low, 1), low + count):
                 await_recv(k["zrecv"].at[i], k["dz_s"].at[i], k["dz_r"].at[i], {"tp": other})
-        for i in range(1, 4):
+        for i in (3, 1, 2):
             there = lax.rem(y + XORD[i], NY)
             src = k["zrecv"].at[pl.ds(low, count), there]
             start(src, part_of(0, i, g), k["dy_s"].at[g, i], k["dy_r"].at[g, i], {"y": there})
@@ -428,33 +437,32 @@
                 await_recv(part_of(0, i, g), k["dy_s"].at[g, i], k["dy_r"].at[g, i], {"tp": other})
                 send_x(i, g)
         send_core(0, g)
-        with jax.named_scope(f"w_dx0{g}"):
-            wait_x(0, 0, g)
+        if not g:
+            with jax.named_scope("w_dx0"):
+                wait_x(0, 0, 0)
     with jax.named_scope("w_dxr"):
-        for g in range(2):
-            wait_x(0, 1, g)
-            wait_x(1, 2, g)
-            wait_x(1, 3, g)
+        wait_x(0, 1, 0)
+        wait_x(1, 2, 0)
+        wait_x(1, 3, 0)
     with jax.named_scope("w_dxe"):
-        for g in range(2):
-            wait_x(0, 2, g)
-            wait_x(0, 3, g)
-            send_core(1, g)
-            wait_x(1, 0, g)
-            wait_x(1, 1, g)
-            send_core(2, g)
-    with jax.named_scope("w_dxl"):
-        for g in range(2):
-            for yi in range(4):
-                await_recv(part_of(3, yi, g), k["dl_s"].at[g, yi], k["dl_r"].at[g, yi], {"tp": other})
-            send_core(3, g)
+        for yi in (2, 3):
+            wait_x(0, yi, 0)
+        send_core(1, 0)
+        for yi in (0, 1):
+            wait_x(1, yi, 0)
+        send_core(2, 0)
+        for n in range(2):
+            for yi in range(NY):
+                wait_x(n, yi, 1)
+            send_core(1 + n, 1)
     with jax.named_scope("w_we"):
         for i in range(14, 19):
             loads[i].wait()
 
     turn = iota(square, 1) == iota(square, 0) % 16 * Q + iota(square, 0) // 16
     turn = jnp.where(turn, 1.0, 0.0).astype(BF)
-    for xi in range(NX):
+
+    def to_rows(xi):
         with jax.named_scope(f"w_dt{xi}"):
             for g in range(2):
                 ref = k["fb"].at[other, xi, :, pl.ds(*GROUPS[g])]
@@ -465,13 +473,15 @@
             at = (xi * NY + yi) * 16
             for q in range(Q):
                 k["ab"][at : at + 16, q * 256 : q * 256 + 256] = turned[q * 16 : q * 16 + 16]
-    gate_act = dot(k["ab"][...], k["wg"][...].reshape(D, FD))
-    upper = dot(k["ab"][...], k["wu"][...].reshape(D, FD))
-    k["ib"][...] = (jax.nn.silu(gate_act) * upper).astype(BF)
+
+    def up(low, high):
+        rows = k["ab"][low:high]
+        gate_act = dot(rows, k["wg"][...].reshape(D, FD))
+        upper = dot(rows, k["wu"][...].reshape(D, FD))
+        k["ib"][low:high] = (jax.nn.silu(gate_act) * upper).astype(BF)
 
     theirs = pl.ds(pl.multiple_of(other * H, H), H)
     ours = pl.ds(pl.multiple_of(tp * H, H), H)
-    ahead, behind = {"x": lax.rem(x + 1, NX)}, {"x": lax.rem(x + 3, NX)}
 
     def down(xi):
         inner = k["ib"][xi * 64 : xi * 64 + 64]
@@ -484,45 +494,42 @@
             await_recv(k["hr"].at[xi], k["ht_s"].at[xi], k["ht_r"].at[xi], {"tp": other})
         return k["own"][xi] + k["hr"][xi].astype(F32)
 
-    def send_sum(xi, half, rows):
-        n = 2 - xi
-        k["xsend"][xi, half] = rows.astype(BF)
-        start(
-            k["xsend"].at[xi, half],
-            k["xrecv"].at[n, half],
-            k["rx_s"].at[n, half],
-            k["rx_r"].at[n, half],
-            (ahead, behind)[n],
-        )
-
+    def send_sum(xi):
+        where = {"x": lax.rem(x - XORD[xi] + NX, NX)}
+        total = whole(xi).astype(BF)
+        for half in (1, 0):
+            k["xsend"][xi, half] = total[half * 32 : half * 32 + 32]
+            src, dst = k["xsend"].at[xi, half], k["xrecv"].at[xi, half]
+            start(src, dst, k["rx_s"].at[xi, half], k["rx_r"].at[xi, half], where)
+
+    for xi in range(3):
+        to_rows(xi)
+    up(0, 192)
+    with jax.named_scope("w_dxl"):
+        for yi in range(NY):
+            await_recv(part_of(3, yi, 0), k["dl_s"].at[0, yi], k["dl_r"].at[0, yi], {"tp": other})
+        send_core(3, 0)
+        for yi in range(NY):
+            wait_x(2, yi, 1)
+        send_core(3, 1)
+    down(1)
+    down(2)
+    to_rows(3)
+    up(192, 256)
     down(3)
-    down(2)
-    far = whole(3)
-    for half in range(2):
-        k["xsend"][3, half] = far[half * 32 : half * 32 + 32].astype(BF)
-        src, dst = k["xsend"].at[3, half], k["rl"].at[half]
-        start(src, dst, k["rl_s"].at[half], k["rl_r"].at[half], (ahead, behind)[half])
-    down(1)
-    next_sum = whole(2)
-    send_sum(2, 1, next_sum[32:])
+    send_sum(1)
+    send_sum(2)
+    send_sum(3)
     down(0)
-    last_sum = whole(1)
-    send_sum(1, 0, last_sum[:32])
-    with jax.named_scope("w_rl0"):
-        await_recv(k["rl"].at[0], k["rl_s"].at[0], k["rl_r"].at[0], {"tp": other})
-    send_sum(2, 0, next_sum[:32] + k["rl"][0].astype(F32))
-    with jax.named_scope("w_rl1"):
-        await_recv(k["rl"].at[1], k["rl_s"].at[1], k["rl_r"].at[1], {"tp": other})
-    send_sum(1, 1, last_sum[32:] + k["rl"][1].astype(F32))
     home = whole(0)
     back = iota(square, 0) == iota(square, 1) % 16 * Q + iota(square, 1) // 16
     back = jnp.where(back, 1.0, 0.0).astype(BF)
     for half in (1, 0):
         with jax.named_scope(f"w_rx{half}"):
-            for n in range(2):
+            for n in range(1, 4):
                 await_recv(k["xrecv"].at[n, half], k["rx_s"].at[n, half], k["rx_r"].at[n, half], {"tp": other})
         rows = home[half * 32 : half * 32 + 32]
-        rows = (rows + k["xrecv"][0, half].astype(F32) + k["xrecv"][1, half].astype(F32)).astype(BF)
+        rows = sum((k["xrecv"][n, half].astype(F32) for n in range(1, 4)), rows).astype(BF)
         for yi in (3, 2) if half else (1, 0):
             part = rows[yi % 2 * 16 : yi % 2 * 16 + 16]
             part = jnp.concatenate([part[:, q * LANES : (q + 1) * LANES] for q in range(Q)], axis=0)
@@ -538,7 +545,7 @@
             for yi in (2, 3) if half else (1,):
                 await_recv(k["ry"].at[yi], k["ry_s"].at[yi], k["ry_r"].at[yi], {"tp": other})
         pair = pl.ds(2 * half, 2)
-        for i in range(1, 8):
+        for i in range(7, 0, -1):
             there = lax.rem(z - ZORD[i] + NZ, NZ)
             start(
                 k["ry"].at[pair, i], k["rz"].at[z, pair], k["rz_s"].at[half, i], k["rz_r"].at[half, i], {"z": there}
@@ -553,16 +560,10 @@
     returned = k["rz"][...].reshape(EXPERTS * 16, LANES).astype(F32)
     mix = dot(k["pw"][...], returned, ((0,), (0,)), HIGHEST)
     expert_mix = jnp.concatenate([mix[q * S : (q + 1) * S] for q in range(Q)], axis=1)
-    k["ns"][...] = (mid_values + expert_mix).astype(BF)
-    store_stream = pltpu.make_async_copy(k["ns"], o_stream, k["stores"].at[2])
-    store_stream.start()
-
+    o_stream[...] = (mid_values + expert_mix).astype(BF)
     for c in sent:
         c.wait_send()
     sends_done("ss", "ra", "a_s", "a_r")
-    store_conv.wait()
-    store_hidden.wait()
-    store_stream.wait()
 
 
 def handed_on(*refs):
@@ -575,6 +576,7 @@
     decay_logit, output_weight, second_gain, routes, route_weight, expert_gate, expert_up, expert_down,
 ):
     shapes = scratch_shapes()
+    vmem = pl.BlockSpec(memory_space=pltpu.VMEM)
     anywhere = pl.BlockSpec(memory_space=pl.ANY)
     outs = pl.pallas_call(
         kernel,
@@ -585,7 +587,7 @@
             jax.ShapeDtypeStruct((3, S, H), BF),
         ),
         in_specs=[anywhere] * 17,
-        out_specs=(anywhere,) * 3,
+        out_specs=(vmem,) * 3,
         scratch_shapes=[shapes[n] for n in NAMES],
         compiler_params=pltpu.CompilerParams(
             collective_id=0, has_side_effects=True, vmem_limit_bytes=60 * 1024 * 1024
@@ -609,7 +611,6 @@
         expert_up.reshape(2, Q, LANES, FD),
         expert_down,
     )
-    vmem = pl.BlockSpec(memory_space=pltpu.VMEM)
     new_stream, new_hidden, new_conv = pl.pallas_call(
         handed_on,
         name="handed_on",

time: 84.2 us -> 78.5 us (0.932); the launches traced: 83 us -> 78.4 us
  Pallas kernels: 82.4 us -> 77.8 us
    pallas_call x1, Pallas kernels: 80.7 us -> 76.2 us  [per_device(): pl.pallas_call(kernel, name='layer', out_shape=(jax.ShapeDtypeStruct((S,...]
where the time goes in v3:
time: 78.5 us; the launch traced here: 78.4 us
  Pallas kernels  77.8 us (99%)
    pallas_call x1, Pallas kernels, per_device(): pl.pallas_call(kernel, name='layer', out_shape=(jax.ShapeDtypeStruct((S,...  76.2 us
    pallas_call x1, Pallas kernels, per_device(): pl.pallas_call(handed_on, name='handed_on', out_shape=tuple((jax.ShapeDty...  1.63 us

profile of v3, /device:TPU:2, one launch (start us, length us, event | category | flops | bytes accessed | tf_op | source)
XLA Modules:
  0.0 78.4 jit_solution(4893164654734308686)
XLA Ops:
  0.6 76.2 %layer.1 = (bf16[16,1024]{1,0:T(8,128)(2,1)}, f32[16,1024]{1,0:T(8,128)}, bf16[3,16,1024]{2,1,0:T(8,128)(2,1)}) custom-call(bf16[16,1024]{1,0:T(8,128)(2,1)} %refs_0_.1, f32[16,1024]{1,0:T(8,128)} %refs_1_.1, bf16[3,16,1024]{2,1,0:T(8,128)(2,1)} %bitcast.18, f32[1,1024]{1,0:T(1,128)} %bitcast.22, bf16[16,1024]{1,0:T(8,128)(2,1)} %bitcast.19, ...), custom_call_target="tpu_custom_call" | custom-call | tf_op jit(solution)/shard_map/layer/pallas_call | solution.py:581
  76.8 1.6 %handed_on.1 = (bf16[16,1024]{1,0:T(8,128)(2,1)}, f32[16,1024]{1,0:T(8,128)}, bf16[3,16,1024]{2,1,0:T(8,128)(2,1)}) custom-call(bf16[16,1024]{1,0:T(8,128)(2,1)} %get-tuple-element.9.refs_0_, f32[16,1024]{1,0:T(8,128)} %get-tuple-element.10.refs_1_, bf16[3,16,1024]{2,1,0:T(8,128)(2,1)} %get-tuple-element.11.refs_2_), custom_call_target="tpu_custom_call" | custom-call | tf_op jit(solution)/shard_map/handed_on/pallas_call | solution.py:614

commit v4 on v3

--- a/solution.py
+++ b/solution.py
@@ -20,6 +20,50 @@
 LANES, Q = 128, 8
 EXPERTS, CAP = 32, 2
 HIGHEST = lax.Precision.HIGHEST
+
+
+SENDS = 32
+
+
+def semaphores():
+    first = {
+        "load": [(i,) for i in range(19)],
+        "t": [(i,) for i in range(4)],
+        "w": [(i, d) for i in range(5) for d in (1, 2, 3)],
+        "x": [(d,) for d in range(8)],
+        "oz": [(d,) for d in range(8)],
+        "ox": [(n, d) for n in range(2) for d in range(8)],
+        "ol": [(d,) for d in range(8)],
+        "m": [(d,) for d in (1, 2, 3)],
+        "b": [(n, d) for n in range(2) for d in range(4) if n or d],
+    }
+    at = {}
+    for name, indices in first.items():
+        for index in indices:
+            at[(name, *index)] = len(at)
+    count = len(at)
+
+    def share(keys, *names):
+        free = [at[(name, *index)] for name in names for index in first[name]]
+        for key, i in zip(keys, free, strict=False):
+            at[key] = i
+        return free[len(keys) :]
+
+    groups, halves = (0, 1), (0, 1)
+    along = [("dz", i) for i in range(1, 8)] + [("dy", g, i) for g in groups for i in (1, 2, 3)]
+    left = share(along, "w")
+    left += [at[("load", i)] for i in range(9, 14)] + [at[("t", 0)]]
+    for key, i in zip([("dt", xi, g) for xi in range(4) for g in groups], left, strict=True):
+        at[key] = i
+    rows = [("dx", n, yi, 0) for n in range(2) for yi in range(4)] + [("dx", n, yi, 1) for n in range(3) for yi in range(4)]
+    share(rows + [("dl", 0, yi) for yi in range(4)], "x", "oz", "load")
+    back = [("ht", xi) for xi in range(4)] + [("rx", xi, half) for xi in (1, 2, 3) for half in halves]
+    back += [("ry", yi) for yi in (1, 2, 3)] + [("rz", half, i) for half in halves for i in range(1, 8)]
+    assert not share(back, "ox", "ol", "m")
+    return at, count
+
+
+AT, COUNT = semaphores()
 
 
 def scratch_shapes():
@@ -67,25 +111,11 @@
         ysend=vm((NY, NZ, 16, LANES), BF),
         ry=vm((NY, NZ, 16, LANES), BF),
         rz=vm((NZ, NY, 16, LANES), BF),
-        loads=dma((24,)),
-        x_s=dma((8,)), x_r=dma((8,)),
-        m_s=dma((8,)), m_r=dma((8,)),
-        w_s=dma((5, 4)), w_r=dma((5, 4)),
-        oz_s=dma((8,)), oz_r=dma((8,)),
-        ox_s=dma((2, 8)), ox_r=dma((2, 8)),
-        ol_s=dma((8,)), ol_r=dma((8,)),
-        t_s=dma((4,)), t_r=dma((4,)),
-        a_s=dma((8,)), a_r=dma((4,)),
-        b_s=dma((2, 4)), b_r=dma((2, 4)),
-        dz_s=dma((8,)), dz_r=dma((8,)),
-        dy_s=dma((2, 4)), dy_r=dma((2, 4)),
-        dx_s=dma((3, 4, 2)), dx_r=dma((3, 4, 2)),
-        dl_s=dma((2, 4)), dl_r=dma((2, 4)),
-        dt_s=dma((4, 2)), dt_r=dma((4, 2)),
-        ht_s=dma((4,)), ht_r=dma((4,)),
-        rx_s=dma((4, 2)), rx_r=dma((4, 2)),
-        ry_s=dma((4,)), ry_r=dma((4,)),
-        rz_s=dma((2, 8)), rz_r=dma((2, 8)),
+        sends=dma((SENDS,)),
+        a_s=dma((8,)),
+        a_r=dma((4,)),
+        p_s=dma((1,)),
+        r=dma((COUNT,)),
     )
 
 
@@ -141,17 +171,23 @@
         (eg.at[0], k["wg"].at[:, 0]), (eg.at[1], k["wg"].at[:, 1]),
         (eu.at[0], k["wu"].at[:, 0]), (eu.at[1], k["wu"].at[:, 1]), (ed, k["wd"]),
     ]
-    loads = [pltpu.make_async_copy(s, t, k["loads"].at[i]) for i, (s, t) in enumerate(plan)]
+    loads = [pltpu.make_async_copy(s, t, k["r"].at[AT[("load", i)]]) for i, (s, t) in enumerate(plan)]
     for c in loads:
         c.start()
 
-    def start(src, dst, ssem, rsem, where):
-        c = remote(src, dst, ssem, rsem, where)
+    def sem(name, *index):
+        return k["r"].at[AT[(name, *index)]]
+
+    def start(src, dst, rsem, where):
+        n = len(sent)
+        if n >= SENDS:
+            sent[n - SENDS].wait_send()
+        c = remote(src, dst, k["sends"].at[n % SENDS], rsem, where)
         c.start()
         sent.append(c)
 
-    def await_recv(ref, ssem, rsem, where):
-        remote(ref, ref, ssem, rsem, where).wait_recv()
+    def await_recv(ref, rsem, where):
+        remote(ref, ref, k["sends"].at[0], rsem, where).wait_recv()
 
     loads[0].wait()
     loads[1].wait()
@@ -207,10 +243,10 @@
 
     def push(ref, i, along):
         for d in ORDER[4]:
-            start(ref, ref, k["w_s"].at[i, d], k["w_r"].at[i, d], along(d))
+            start(ref, ref, sem("w", i, d), along(d))
 
     def pull(ref, i, d):
-        await_recv(ref, k["w_s"].at[i, d], k["w_r"].at[i, d], {"tp": other})
+        await_recv(ref, sem("w", i, d), {"tp": other})
 
     push(block(0, 0), 4, along_b)
     push(block(0, 0), 0, along_a)
@@ -223,39 +259,39 @@
     def slot(ref, d):
         return ref.at[lax.rem(z - d + NZ, NZ)]
 
-    def column_send(ref, ssem, rsem):
+    def column_send(ref, name):
         for d in near:
-            start(ref.at[z], ref.at[z], ssem.at[d], rsem.at[d], along_z(d))
-
-    def column_relay(ref, ssem, rsem):
+            start(ref.at[z], ref.at[z], sem(name, d), along_z(d))
+
+    def column_relay(ref, name):
         for n, d in enumerate((2, 6)):
             got, piece = slot(ref, d), slot(ref, d).at[:, lanes[n]]
-            await_recv(got, ssem.at[d], rsem.at[d], {"tp": other})
-            start(piece, piece, ssem.at[(0, 4)[n]], rsem.at[(0, 4)[n]], along_z(d))
-            start(got, got, ssem.at[(3, 5)[n]], rsem.at[(3, 5)[n]], along_z((1, 7)[n]))
-
-    def column_end(ref, ssem, rsem):
+            await_recv(got, sem(name, d), {"tp": other})
+            start(piece, piece, sem(name, (0, 4)[n]), along_z(d))
+            start(got, got, sem(name, (3, 5)[n]), along_z((1, 7)[n]))
+
+    def column_end(ref, name):
         for d in (3, 5):
-            await_recv(slot(ref, d), ssem.at[d], rsem.at[d], {"tp": other})
+            await_recv(slot(ref, d), sem(name, d), {"tp": other})
         for n in range(2):
-            await_recv(slot(ref, 4).at[:, lanes[n]], ssem.at[(0, 4)[n]], rsem.at[(0, 4)[n]], {"tp": other})
-
-    rows_column = (k["xs"], k["x_s"], k["x_r"])
-    weight_column = (k["wo"].at[x], k["oz_s"], k["oz_r"])
+            await_recv(slot(ref, 4).at[:, lanes[n]], sem(name, (0, 4)[n]), {"tp": other})
+
+    rows_column = (k["xs"], "x")
+    weight_column = (k["wo"].at[x], "oz")
     column_send(*rows_column)
-    start(k["qs"].at[0], k["qr"].at[0], k["t_s"].at[0], k["t_r"].at[0], {"tp": other})
+    start(k["qs"].at[0], k["qr"].at[0], sem("t", 0), {"tp": other})
     column_send(*weight_column)
     def spread_slot(d):
         for n in range(2):
             ref, where = k["wo"].at[x, lax.rem(z - d + NZ, NZ)], {"x": lax.rem(x + (1, 3)[n], NX)}
-            start(ref, ref, k["ox_s"].at[n, d], k["ox_r"].at[n, d], where)
+            start(ref, ref, sem("ox", n, d), where)
 
     def relay_slot(d):
         for n in range(2):
             ref = k["wo"].at[lax.rem(x + (3, 1)[n], NX), lax.rem(z - d + NZ, NZ)]
-            await_recv(ref, k["ox_s"].at[n, d], k["ox_r"].at[n, d], {"tp": other})
+            await_recv(ref, sem("ox", n, d), {"tp": other})
             if n == (d in (3, 4, 5, 6)):
-                start(ref, ref, k["ol_s"].at[d], k["ol_r"].at[d], {"x": lax.rem(x + (1, 3)[n], NX)})
+                start(ref, ref, sem("ol", d), {"x": lax.rem(x + (1, 3)[n], NX)})
 
     with jax.named_scope("w_b"):
         for i in (1, 3, 2):
@@ -266,12 +302,12 @@
     with jax.named_scope("w_oz"):
         column_relay(*weight_column)
         for d in (1, 7):
-            await_recv(slot(weight_column[0], d), k["oz_s"].at[d], k["oz_r"].at[d], {"tp": other})
+            await_recv(slot(weight_column[0], d), sem("oz", d), {"tp": other})
         for d in (0, 1, 7, 2, 6):
             spread_slot(d)
     with jax.named_scope("w_xg"):
         for d in (1, 7):
-            await_recv(slot(k["xs"], d), k["x_s"].at[d], k["x_r"].at[d], {"tp": other})
+            await_recv(slot(k["xs"], d), sem("x", d), {"tp": other})
         column_end(*rows_column)
     with jax.named_scope("w_oze"):
         column_end(*weight_column)
@@ -296,13 +332,13 @@
         @pl.when(tp != z // 4)
         def _():
             k[ps][...] = part.astype(BF)
-            c = remote(k[ps], k[pr], k["t_s"].at[t], k["t_r"].at[t], {"tp": other})
+            c = remote(k[ps], k[pr], k["p_s"].at[0], sem("t", t), {"tp": other})
             c.start()
             c.wait_send()
 
         @pl.when(tp == z // 4)
         def _():
-            await_recv(k[pr], k["t_s"].at[t], k["t_r"].at[t], {"tp": other})
+            await_recv(k[pr], sem("t", t), {"tp": other})
             total = (part + k[pr][...].astype(F32)).astype(BF)
             k[ss][...] = total.reshape(NZ, S, width)
             mine = lax.rem(z, 4)
@@ -315,7 +351,7 @@
         for i in range(4):
             @pl.when(4 * tp + i != z)
             def _():
-                await_recv(k[land].at[i], k[sends].at[0], k[lands].at[i], {"tp": other})
+                await_recv(k[land].at[i], k[lands].at[i], {"tp": other})
 
     def sends_done(ss, land, sends, lands):
         @pl.when(tp == z // 4)
@@ -329,7 +365,7 @@
                 relay_slot(d)
 
     project("xs", (0, 1), 512, "ps", "pr", "ss", "ra", 1, "a_s", "a_r", output_weight)
-    await_recv(k["qr"].at[0], k["t_s"].at[0], k["t_r"].at[0], {"tp": other})
+    await_recv(k["qr"].at[0], sem("t", 0), {"tp": other})
     row_scale = lax.rsqrt((k["qs"][0] + k["qr"][0])[:, 0:1] / D + EPSILON)
     forward = (jnp.concatenate([k["ra"][i, :, 0:256] for i in range(4)], axis=1).astype(F32) * row_scale).astype(BF)
     branch = (jnp.concatenate([k["ra"][i, :, 256:512] for i in range(4)], axis=1).astype(F32) * row_scale).astype(BF)
@@ -356,16 +392,16 @@
     o_hidden[...] = new_hidden
     k["ms"][y] = (jax.nn.gelu(branch.astype(F32)) * new_hidden).astype(BF)
     for d in ORDER[4]:
-        start(k["ms"].at[y], k["ms"].at[y], k["m_s"].at[d], k["m_r"].at[d], {"y": lax.rem(y + d, NY)})
+        start(k["ms"].at[y], k["ms"].at[y], sem("m", d), {"y": lax.rem(y + d, NY)})
     with jax.named_scope("w_ox2"):
         for d in (3, 5, 4):
             relay_slot(d)
         for d in range(NZ):
             ref = k["wo"].at[lax.rem(x + 2, NX), lax.rem(z - d + NZ, NZ)]
-            await_recv(ref, k["ol_s"].at[d], k["ol_r"].at[d], {"tp": other})
+            await_recv(ref, sem("ol", d), {"tp": other})
     with jax.named_scope("w_mg"):
         for d in ORDER[4]:
-            await_recv(k["ms"].at[lax.rem(y - d + NY, NY)], k["m_s"].at[d], k["m_r"].at[d], {"tp": other})
+            await_recv(k["ms"].at[lax.rem(y - d + NY, NY)], sem("m", d), {"tp": other})
     lhs = k["ms"][...].reshape(NY * S, H)
     for h in range(2):
         out_columns = jnp.concatenate([k["wo"][j, 4 * h + i] for i in range(4) for j in range(NX)], axis=0)
@@ -376,14 +412,14 @@
         for n, core in enumerate((tp, other)):
             if d or n:
                 where = {"y": there, "tp": core}
-                start(k["ps2"].at[core, there], k["rb"].at[n, y], k["b_s"].at[n, d], k["b_r"].at[n, d], where)
+                start(k["ps2"].at[core, there], k["rb"].at[n, y], sem("b", n, d), where)
     k["rb"][0, y] = k["ps2"][tp, y]
     with jax.named_scope("w_rb"):
         for d in ORDER[4] + (0,):
             for n in range(2):
                 if d or n:
                     ref = k["rb"].at[n, lax.rem(y - d + NY, NY)]
-                    await_recv(ref, k["b_s"].at[n, d], k["b_r"].at[n, d], {"tp": other})
+                    await_recv(ref, sem("b", n, d), {"tp": other})
     landed = k["rb"][0].astype(F32) + k["rb"][1].astype(F32)
     out_terms = jnp.concatenate(
         [landed[j, :, i * 64 : i * 64 + 64] for i in range(4) for j in range(NY)], axis=1
@@ -391,8 +427,8 @@
     middle = (values + out_terms).astype(BF)
     mid_values = middle.astype(F32)
     k["qs"][1] = jnp.broadcast_to(jnp.sum(mid_values * mid_values, axis=1, keepdims=True), (S, LANES))
-    start(k["qs"].at[1], k["qr"].at[1], k["t_s"].at[3], k["t_r"].at[3], {"tp": other})
-    await_recv(k["qr"].at[1], k["t_s"].at[3], k["t_r"].at[3], {"tp": other})
+    start(k["qs"].at[1], k["qr"].at[1], sem("t", 3), {"tp": other})
+    await_recv(k["qr"].at[1], sem("t", 3), {"tp": other})
     mid_scale = lax.rsqrt((k["qs"][1] + k["qr"][1])[:, 0:1] / D + EPSILON)
     normed = (mid_values * mid_scale * k["g2v"][...]).astype(BF)
 
@@ -400,7 +436,7 @@
     k["zsend"][...] = dot(k["pm"][...], stacked).astype(BF).reshape(NZ, NY, 16, LANES)
     for i in range(7, 0, -1):
         there = lax.rem(z + ZORD[i], NZ)
-        start(k["zsend"].at[there], k["zrecv"].at[i], k["dz_s"].at[i], k["dz_r"].at[i], {"z": there})
+        start(k["zsend"].at[there], k["zrecv"].at[i], sem("dz", i), {"z": there})
     k["zrecv"][0] = k["zsend"][z]
 
     def part_of(xi, yi, g, h=tp):
@@ -409,32 +445,32 @@
     def send_x(yi, g):
         for n in (2, 0, 1) if g else (0, 1):
             where = {"x": lax.rem(x + (1, 3, 2)[n], NX)}
-            start(part_of(0, yi, g), part_of(1 + n, yi, g), k["dx_s"].at[n, yi, g], k["dx_r"].at[n, yi, g], where)
+            start(part_of(0, yi, g), part_of(1 + n, yi, g), sem("dx", n, yi, g), where)
 
     def wait_x(n, yi, g):
-        await_recv(part_of(1 + n, yi, g), k["dx_s"].at[n, yi, g], k["dx_r"].at[n, yi, g], {"tp": other})
+        await_recv(part_of(1 + n, yi, g), sem("dx", n, yi, g), {"tp": other})
         if yi // 2 == n and not g:
             where = {"x": lax.rem(x + (1, 3)[n], NX)}
-            start(part_of(1 + n, yi, g), part_of(3, yi, g), k["dl_s"].at[g, yi], k["dl_r"].at[g, yi], where)
+            start(part_of(1 + n, yi, g), part_of(3, yi, g), sem("dl", g, yi), where)
 
     def send_core(xi, g):
         ref = k["fb"].at[tp, xi, :, pl.ds(*GROUPS[g])]
-        start(ref, ref, k["dt_s"].at[xi, g], k["dt_r"].at[xi, g], {"tp": other})
+        start(ref, ref, sem("dt", xi, g), {"tp": other})
 
     for g, (low, count) in enumerate(GROUPS):
         with jax.named_scope(f"w_dz{g}"):
             for i in range(max(low, 1), low + count):
-                await_recv(k["zrecv"].at[i], k["dz_s"].at[i], k["dz_r"].at[i], {"tp": other})
+                await_recv(k["zrecv"].at[i], sem("dz", i), {"tp": other})
         for i in (3, 1, 2):
             there = lax.rem(y + XORD[i], NY)
             src = k["zrecv"].at[pl.ds(low, count), there]
-            start(src, part_of(0, i, g), k["dy_s"].at[g, i], k["dy_r"].at[g, i], {"y": there})
+            start(src, part_of(0, i, g), sem("dy", g, i), {"y": there})
         k["fb"][tp, 0, 0, low : low + count] = k["zrecv"][low : low + count, y]
         send_x(0, g)
     for g in range(2):
         with jax.named_scope(f"w_dy{g}"):
             for i in range(1, 4):
-                await_recv(part_of(0, i, g), k["dy_s"].at[g, i], k["dy_r"].at[g, i], {"tp": other})
+                await_recv(part_of(0, i, g), sem("dy", g, i), {"tp": other})
                 send_x(i, g)
         send_core(0, g)
         if not g:
@@ -466,7 +502,7 @@
         with jax.named_scope(f"w_dt{xi}"):
             for g in range(2):
                 ref = k["fb"].at[other, xi, :, pl.ds(*GROUPS[g])]
-                await_recv(ref, k["dt_s"].at[xi, g], k["dt_r"].at[xi, g], {"tp": other})
+                await_recv(ref, sem("dt", xi, g), {"tp": other})
         for yi in range(NY):
             pair = jnp.concatenate([k["fb"][h, xi, yi].reshape(LANES, LANES) for h in range(2)], axis=1)
             turned = dot(turn, pair).astype(BF)
@@ -486,12 +522,12 @@
     def down(xi):
         inner = k["ib"][xi * 64 : xi * 64 + 64]
         k["hs"][xi] = dot(inner, k["wd"][:, theirs]).astype(BF)
-        start(k["hs"].at[xi], k["hr"].at[xi], k["ht_s"].at[xi], k["ht_r"].at[xi], {"tp": other})
+        start(k["hs"].at[xi], k["hr"].at[xi], sem("ht", xi), {"tp": other})
         k["own"][xi] = dot(inner, k["wd"][:, ours])
 
     def whole(xi):
         with jax.named_scope(f"w_ht{xi}"):
-            await_recv(k["hr"].at[xi], k["ht_s"].at[xi], k["ht_r"].at[xi], {"tp": other})
+            await_recv(k["hr"].at[xi], sem("ht", xi), {"tp": other})
         return k["own"][xi] + k["hr"][xi].astype(F32)
 
     def send_sum(xi):
@@ -500,14 +536,14 @@
         for half in (1, 0):
             k["xsend"][xi, half] = total[half * 32 : half * 32 + 32]
             src, dst = k["xsend"].at[xi, half], k["xrecv"].at[xi, half]
-            start(src, dst, k["rx_s"].at[xi, half], k["rx_r"].at[xi, half], where)
+            start(src, dst, sem("rx", xi, half), where)
 
     for xi in range(3):
         to_rows(xi)
     up(0, 192)
     with jax.named_scope("w_dxl"):
         for yi in range(NY):
-            await_recv(part_of(3, yi, 0), k["dl_s"].at[0, yi], k["dl_r"].at[0, yi], {"tp": other})
+            await_recv(part_of(3, yi, 0), sem("dl", 0, yi), {"tp": other})
         send_core(3, 0)
         for yi in range(NY):
             wait_x(2, yi, 1)
@@ -527,7 +563,7 @@
     for half in (1, 0):
         with jax.named_scope(f"w_rx{half}"):
             for n in range(1, 4):
-                await_recv(k["xrecv"].at[n, half], k["rx_s"].at[n, half], k["rx_r"].at[n, half], {"tp": other})
+                await_recv(k["xrecv"].at[n, half], sem("rx", n, half), {"tp": other})
         rows = home[half * 32 : half * 32 + 32]
         rows = sum((k["xrecv"][n, half].astype(F32) for n in range(1, 4)), rows).astype(BF)
         for yi in (3, 2) if half else (1, 0):
@@ -537,18 +573,18 @@
             if yi:
                 k["ysend"][yi] = part
                 where = {"y": lax.rem(y - XORD[yi] + NY, NY)}
-                start(k["ysend"].at[yi], k["ry"].at[yi], k["ry_s"].at[yi], k["ry_r"].at[yi], where)
+                start(k["ysend"].at[yi], k["ry"].at[yi], sem("ry", yi), where)
             else:
                 k["ry"][0] = part
     for half in (1, 0):
         with jax.named_scope(f"w_ry{half}"):
             for yi in (2, 3) if half else (1,):
-                await_recv(k["ry"].at[yi], k["ry_s"].at[yi], k["ry_r"].at[yi], {"tp": other})
+                await_recv(k["ry"].at[yi], sem("ry", yi), {"tp": other})
         pair = pl.ds(2 * half, 2)
         for i in range(7, 0, -1):
             there = lax.rem(z - ZORD[i] + NZ, NZ)
             start(
-                k["ry"].at[pair, i], k["rz"].at[z, pair], k["rz_s"].at[half, i], k["rz_r"].at[half, i], {"z": there}
+                k["ry"].at[pair, i], k["rz"].at[z, pair], sem("rz", half, i), {"z": there}
             )
         k["rz"][z, 2 * half : 2 * half + 2] = k["ry"][2 * half : 2 * half + 2, 0]
     with jax.named_scope("w_rz"):
@@ -556,12 +592,12 @@
             pair = pl.ds(2 * half, 2)
             for i in range(1, 8):
                 ref = k["rz"].at[lax.rem(z + ZORD[i], NZ), pair]
-                await_recv(ref, k["rz_s"].at[half, i], k["rz_r"].at[half, i], {"tp": other})
+                await_recv(ref, sem("rz", half, i), {"tp": other})
     returned = k["rz"][...].reshape(EXPERTS * 16, LANES).astype(F32)
     mix = dot(k["pw"][...], returned, ((0,), (0,)), HIGHEST)
     expert_mix = jnp.concatenate([mix[q * S : (q + 1) * S] for q in range(Q)], axis=1)
     o_stream[...] = (mid_values + expert_mix).astype(BF)
-    for c in sent:
+    for c in sent[-SENDS:]:
         c.wait_send()
     sends_done("ss", "ra", "a_s", "a_r")
 

time: 78.5 us -> 76.3 us (0.972)
  Pallas kernels: 77.8 us -> 75.6 us
    pallas_call x1, Pallas kernels: 76.2 us -> 73.9 us  [per_device(): pl.pallas_call(kernel, name='layer', out_shape=(jax.ShapeDtypeStruct((S,...]
where the time goes in v4:
time: 76.3 us; the launch traced here: 76.2 us
  Pallas kernels  75.6 us (99%)
    pallas_call x1, Pallas kernels, per_device(): pl.pallas_call(kernel, name='layer', out_shape=(jax.ShapeDtypeStruct((S,...  73.9 us
    pallas_call x1, Pallas kernels, per_device(): pl.pallas_call(handed_on, name='handed_on', out_shape=tuple((jax.ShapeDty...  1.63 us

profile of v4, /device:TPU:2, one launch (start us, length us, event | category | flops | bytes accessed | tf_op | source)
XLA Modules:
  0.0 76.2 jit_solution(2174432932666933335)
XLA Ops:
  0.6 73.9 %layer.1 = (bf16[16,1024]{1,0:T(8,128)(2,1)}, f32[16,1024]{1,0:T(8,128)}, bf16[3,16,1024]{2,1,0:T(8,128)(2,1)}) custom-call(bf16[16,1024]{1,0:T(8,128)(2,1)} %refs_0_.1, f32[16,1024]{1,0:T(8,128)} %refs_1_.1, bf16[3,16,1024]{2,1,0:T(8,128)(2,1)} %bitcast.18, f32[1,1024]{1,0:T(1,128)} %bitcast.22, bf16[16,1024]{1,0:T(8,128)(2,1)} %bitcast.19, ...), custom_call_target="tpu_custom_call" | custom-call | tf_op jit(solution)/shard_map/layer/pallas_call | solution.py:617
  74.6 1.6 %handed_on.1 = (bf16[16,1024]{1,0:T(8,128)(2,1)}, f32[16,1024]{1,0:T(8,128)}, bf16[3,16,1024]{2,1,0:T(8,128)(2,1)}) custom-call(bf16[16,1024]{1,0:T(8,128)(2,1)} %get-tuple-element.9.refs_0_, f32[16,1024]{1,0:T(8,128)} %get-tuple-element.10.refs_1_, bf16[3,16,1024]{2,1,0:T(8,128)(2,1)} %get-tuple-element.11.refs_2_), custom_call_target="tpu_custom_call" | custom-call | tf_op jit(solution)/shard_map/handed_on/pallas_call | solution.py:650

commit v5 on v4

--- a/solution.py
+++ b/solution.py
@@ -13,6 +13,7 @@
 ORDER = {8: (4, 3, 5, 2, 6, 1, 7), 4: (2, 1, 3)}
 ZORD, XORD = (0, 1, 7, 2, 6, 3, 5, 4), (0, 1, 3, 2)
 GROUPS = ((0, 5), (5, 3))
+PLANE = tuple((i, j) for i in (3, 2, 1, 0) for j in (3, 2, 1, 0) if i or j)
 BF, F32 = jnp.bfloat16, jnp.float32
 EPSILON = 1e-6
 DECAY_POWER = 8.0
@@ -36,6 +37,7 @@
         "ol": [(d,) for d in range(8)],
         "m": [(d,) for d in (1, 2, 3)],
         "b": [(n, d) for n in range(2) for d in range(4) if n or d],
+        "more": [(i,) for i in range(5)],
     }
     at = {}
     for name, indices in first.items():
@@ -50,16 +52,14 @@
         return free[len(keys) :]
 
     groups, halves = (0, 1), (0, 1)
-    along = [("dz", i) for i in range(1, 8)] + [("dy", g, i) for g in groups for i in (1, 2, 3)]
-    left = share(along, "w")
-    left += [at[("load", i)] for i in range(9, 14)] + [at[("t", 0)]]
+    left = share([("dz", i) for i in range(1, 8)], "w")
     for key, i in zip([("dt", xi, g) for xi in range(4) for g in groups], left, strict=True):
         at[key] = i
-    rows = [("dx", n, yi, 0) for n in range(2) for yi in range(4)] + [("dx", n, yi, 1) for n in range(3) for yi in range(4)]
-    share(rows + [("dl", 0, yi) for yi in range(4)], "x", "oz", "load")
-    back = [("ht", xi) for xi in range(4)] + [("rx", xi, half) for xi in (1, 2, 3) for half in halves]
-    back += [("ry", yi) for yi in (1, 2, 3)] + [("rz", half, i) for half in halves for i in range(1, 8)]
-    assert not share(back, "ox", "ol", "m")
+    plane = [(xi, yi) for xi in range(4) for yi in range(4) if xi or yi]
+    share([("dp", g, *at_plane) for g in groups for at_plane in plane], "x", "oz", "more", "load")
+    back = [("ht", xi) for xi in range(4)] + [("rx", *at_plane) for at_plane in plane]
+    back += [("rz", half, i) for half in halves for i in range(1, 8)]
+    share(back, "ox", "ol", "m", "b")
     return at, count
 
 
@@ -91,10 +91,11 @@
         pr=vm((NZ * S, 512), BF),
         ss=vm((NZ, S, 512), BF),
         ra=vm((4, S, 512), BF),
-        ps2=vm((2, NY, S, 256), BF),
-        rb=vm((2, NY, S, 256), BF),
-        qs=vm((2, S, LANES), F32),
-        qr=vm((2, S, LANES), F32),
+        ps2=vm((NY, 2, S, 256), BF),
+        svo=vm((S, H), BF),
+        rb=vm((2, NY, 2, S, 256), BF),
+        qs=vm((S, LANES), F32),
+        qr=vm((S, LANES), F32),
         bd=vm((2, 4, 256, 256), BF),
         pm=vm((EXPERTS * 16, LANES), BF),
         pw=vm((EXPERTS * 16, LANES), F32),
@@ -106,12 +107,12 @@
         hs=vm((NX, 64, H), BF),
         hr=vm((NX, 64, H), BF),
         own=vm((NX, 64, H), F32),
-        xsend=vm((NX, 2, 32, H), BF),
-        xrecv=vm((NX, 2, 32, H), BF),
-        ysend=vm((NY, NZ, 16, LANES), BF),
+        xsend=vm((NX, NY, 16, H), BF),
+        xrecv=vm((NX, NY, 16, H), BF),
         ry=vm((NY, NZ, 16, LANES), BF),
         rz=vm((NZ, NY, 16, LANES), BF),
         sends=dma((SENDS,)),
+        spread=dma((2, 8)),
         a_s=dma((8,)),
         a_r=dma((4,)),
         p_s=dma((1,)),
@@ -152,10 +153,11 @@
     sent = []
 
     barrier = pltpu.get_barrier_semaphore()
-    for axis, me in (("z", z), ("y", y), ("x", x)):
-        n = {"z": NZ, "y": NY, "x": NX}[axis]
-        for d in ORDER[n]:
-            pl.semaphore_signal(barrier, inc=1, device_id={axis: lax.rem(me + d, n)}, device_id_type=MESH)
+    for d in ORDER[8]:
+        pl.semaphore_signal(barrier, inc=1, device_id={"z": lax.rem(z + d, NZ)}, device_id_type=MESH)
+    for i, j in PLANE:
+        there = {"y": lax.rem(y + XORD[j], NY), "x": lax.rem(x + XORD[i], NX)}
+        pl.semaphore_signal(barrier, inc=1, device_id=there, device_id_type=MESH)
     for d in ORDER[4]:
         there = {"y": lax.rem(y + d, NY), "tp": other}
         pl.semaphore_signal(barrier, inc=1, device_id=there, device_id_type=MESH)
@@ -193,7 +195,7 @@
     loads[1].wait()
     values = k["sv"][...].astype(F32)
     k["xs"][z] = (values * k["g1v"][...]).astype(BF)
-    k["qs"][0] = jnp.broadcast_to(jnp.sum(values * values, axis=1, keepdims=True), (S, LANES))
+    k["qs"][...] = jnp.broadcast_to(jnp.sum(values * values, axis=1, keepdims=True), (S, LANES))
     loads[5].wait()
     loads[6].wait()
     eye = (iota((64, 256), 1) % 64 == iota((64, 256), 0)).astype(BF)
@@ -228,7 +230,7 @@
     for i in (2, 3, 4):
         loads[i].wait()
     with jax.named_scope("w_bar"):
-        pl.semaphore_wait(barrier, 17)
+        pl.semaphore_wait(barrier, 26)
 
     def along_b(d):
         return {"y": lax.rem(y + d * tp, NY), "x": lax.rem(x + d * other, NX)}
@@ -279,12 +281,22 @@
     rows_column = (k["xs"], "x")
     weight_column = (k["wo"].at[x], "oz")
     column_send(*rows_column)
-    start(k["qs"].at[0], k["qr"].at[0], sem("t", 0), {"tp": other})
+    start(k["qs"], k["qr"], sem("t", 0), {"tp": other})
+    start(k["sv"], k["svo"], sem("t", 3), {"tp": other})
     column_send(*weight_column)
-    def spread_slot(d):
-        for n in range(2):
-            ref, where = k["wo"].at[x, lax.rem(z - d + NZ, NZ)], {"x": lax.rem(x + (1, 3)[n], NX)}
-            start(ref, ref, sem("ox", n, d), where)
+    def spread_slots(ds, core):
+        copies = []
+        for d in ds:
+            for n in range(2):
+                ref, where = k["wo"].at[x, lax.rem(z - d + NZ, NZ)], {"x": lax.rem(x + (1, 3)[n], NX)}
+                copies.append(remote(ref, ref, k["spread"].at[n, d], sem("ox", n, d), where))
+
+        @pl.when(tp == core)
+        def _():
+            for c in copies:
+                c.start()
+
+        return copies
 
     def relay_slot(d):
         for n in range(2):
@@ -303,16 +315,15 @@
         column_relay(*weight_column)
         for d in (1, 7):
             await_recv(slot(weight_column[0], d), sem("oz", d), {"tp": other})
-        for d in (0, 1, 7, 2, 6):
-            spread_slot(d)
+        spread_slots((0, 1, 7, 2, 6), 1)
     with jax.named_scope("w_xg"):
         for d in (1, 7):
             await_recv(slot(k["xs"], d), sem("x", d), {"tp": other})
         column_end(*rows_column)
     with jax.named_scope("w_oze"):
         column_end(*weight_column)
-        for d in (3, 5, 4):
-            spread_slot(d)
+        spread_slots((3, 5, 4), 1)
+        spread_slots((0, 1, 7, 2, 6, 3, 5, 4), 0)
     with jax.named_scope("w_aend"):
         for i in (0, 1, 3, 2):
             for d in (1, 3, 2):
@@ -365,8 +376,8 @@
                 relay_slot(d)
 
     project("xs", (0, 1), 512, "ps", "pr", "ss", "ra", 1, "a_s", "a_r", output_weight)
-    await_recv(k["qr"].at[0], sem("t", 0), {"tp": other})
-    row_scale = lax.rsqrt((k["qs"][0] + k["qr"][0])[:, 0:1] / D + EPSILON)
+    await_recv(k["qr"], sem("t", 0), {"tp": other})
+    row_scale = lax.rsqrt((k["qs"][...] + k["qr"][...])[:, 0:1] / D + EPSILON)
     forward = (jnp.concatenate([k["ra"][i, :, 0:256] for i in range(4)], axis=1).astype(F32) * row_scale).astype(BF)
     branch = (jnp.concatenate([k["ra"][i, :, 256:512] for i in range(4)], axis=1).astype(F32) * row_scale).astype(BF)
     for i in range(9, 14):
@@ -406,35 +417,38 @@
     for h in range(2):
         out_columns = jnp.concatenate([k["wo"][j, 4 * h + i] for i in range(4) for j in range(NX)], axis=0)
         part = dot(lhs, out_columns, ((1,), (1,)))
-        k["ps2"][h] = part.astype(BF).reshape(NY, S, 256)
+        k["ps2"][:, h] = part.astype(BF).reshape(NY, S, 256)
     for d in ORDER[4] + (0,):
         there = lax.rem(y + d, NY)
         for n, core in enumerate((tp, other)):
             if d or n:
                 where = {"y": there, "tp": core}
-                start(k["ps2"].at[core, there], k["rb"].at[n, y], sem("b", n, d), where)
-    k["rb"][0, y] = k["ps2"][tp, y]
+                start(k["ps2"].at[there], k["rb"].at[n, y], sem("b", n, d), where)
+    k["rb"][0, y] = k["ps2"][y]
     with jax.named_scope("w_rb"):
+        await_recv(k["svo"], sem("t", 3), {"tp": other})
         for d in ORDER[4] + (0,):
             for n in range(2):
                 if d or n:
                     ref = k["rb"].at[n, lax.rem(y - d + NY, NY)]
                     await_recv(ref, sem("b", n, d), {"tp": other})
-    landed = k["rb"][0].astype(F32) + k["rb"][1].astype(F32)
-    out_terms = jnp.concatenate(
-        [landed[j, :, i * 64 : i * 64 + 64] for i in range(4) for j in range(NY)], axis=1
-    )
-    middle = (values + out_terms).astype(BF)
-    mid_values = middle.astype(F32)
-    k["qs"][1] = jnp.broadcast_to(jnp.sum(mid_values * mid_values, axis=1, keepdims=True), (S, LANES))
-    start(k["qs"].at[1], k["qr"].at[1], sem("t", 3), {"tp": other})
-    await_recv(k["qr"].at[1], sem("t", 3), {"tp": other})
-    mid_scale = lax.rsqrt((k["qs"][1] + k["qr"][1])[:, 0:1] / D + EPSILON)
+
+    def middle_of(ref, h):
+        landed = k["rb"][0, :, h].astype(F32) + k["rb"][1, :, h].astype(F32)
+        out_terms = jnp.concatenate(
+            [landed[j, :, i * 64 : i * 64 + 64] for i in range(4) for j in range(NY)], axis=1
+        )
+        return (ref[...].astype(F32) + out_terms).astype(BF).astype(F32)
+
+    mid_values = middle_of(k["sv"], tp)
+    theirs_mid = middle_of(k["svo"], other)
+    mid_power = sum(jnp.sum(m * m, axis=1, keepdims=True) for m in (mid_values, theirs_mid)) / D
+    mid_scale = lax.rsqrt(mid_power + EPSILON)
     normed = (mid_values * mid_scale * k["g2v"][...]).astype(BF)
 
     stacked = jnp.concatenate([normed[:, q * LANES : (q + 1) * LANES] for q in range(Q)], axis=0)
     k["zsend"][...] = dot(k["pm"][...], stacked).astype(BF).reshape(NZ, NY, 16, LANES)
-    for i in range(7, 0, -1):
+    for i in range(1, 8):
         there = lax.rem(z + ZORD[i], NZ)
         start(k["zsend"].at[there], k["zrecv"].at[i], sem("dz", i), {"z": there})
     k["zrecv"][0] = k["zsend"][z]
@@ -442,16 +456,9 @@
     def part_of(xi, yi, g, h=tp):
         return k["fb"].at[h, xi, yi, pl.ds(*GROUPS[g])]
 
-    def send_x(yi, g):
-        for n in (2, 0, 1) if g else (0, 1):
-            where = {"x": lax.rem(x + (1, 3, 2)[n], NX)}
-            start(part_of(0, yi, g), part_of(1 + n, yi, g), sem("dx", n, yi, g), where)
-
-    def wait_x(n, yi, g):
-        await_recv(part_of(1 + n, yi, g), sem("dx", n, yi, g), {"tp": other})
-        if yi // 2 == n and not g:
-            where = {"x": lax.rem(x + (1, 3)[n], NX)}
-            start(part_of(1 + n, yi, g), part_of(3, yi, g), sem("dl", g, yi), where)
+    def wait_plane(xi, yi, g):
+        if xi or yi:
+            await_recv(part_of(xi, yi, g), sem("dp", g, xi, yi), {"tp": other})
 
     def send_core(xi, g):
         ref = k["fb"].at[tp, xi, :, pl.ds(*GROUPS[g])]
@@ -461,36 +468,17 @@
         with jax.named_scope(f"w_dz{g}"):
             for i in range(max(low, 1), low + count):
                 await_recv(k["zrecv"].at[i], sem("dz", i), {"tp": other})
-        for i in (3, 1, 2):
-            there = lax.rem(y + XORD[i], NY)
+        for i, j in PLANE:
+            there = lax.rem(y + XORD[j], NY)
             src = k["zrecv"].at[pl.ds(low, count), there]
-            start(src, part_of(0, i, g), sem("dy", g, i), {"y": there})
+            start(src, part_of(i, j, g), sem("dp", g, i, j), {"y": there, "x": lax.rem(x + XORD[i], NX)})
         k["fb"][tp, 0, 0, low : low + count] = k["zrecv"][low : low + count, y]
-        send_x(0, g)
-    for g in range(2):
-        with jax.named_scope(f"w_dy{g}"):
-            for i in range(1, 4):
-                await_recv(part_of(0, i, g), sem("dy", g, i), {"tp": other})
-                send_x(i, g)
-        send_core(0, g)
-        if not g:
-            with jax.named_scope("w_dx0"):
-                wait_x(0, 0, 0)
-    with jax.named_scope("w_dxr"):
-        wait_x(0, 1, 0)
-        wait_x(1, 2, 0)
-        wait_x(1, 3, 0)
-    with jax.named_scope("w_dxe"):
-        for yi in (2, 3):
-            wait_x(0, yi, 0)
-        send_core(1, 0)
-        for yi in (0, 1):
-            wait_x(1, yi, 0)
-        send_core(2, 0)
-        for n in range(2):
-            for yi in range(NY):
-                wait_x(n, yi, 1)
-            send_core(1 + n, 1)
+    for xi in range(3):
+        for g in range(2):
+            with jax.named_scope(f"w_dp{xi}{g}"):
+                for yi in range(NY):
+                    wait_plane(xi, yi, g)
+            send_core(xi, g)
     with jax.named_scope("w_we"):
         for i in range(14, 19):
             loads[i].wait()
@@ -531,23 +519,22 @@
         return k["own"][xi] + k["hr"][xi].astype(F32)
 
     def send_sum(xi):
-        where = {"x": lax.rem(x - XORD[xi] + NX, NX)}
-        total = whole(xi).astype(BF)
-        for half in (1, 0):
-            k["xsend"][xi, half] = total[half * 32 : half * 32 + 32]
-            src, dst = k["xsend"].at[xi, half], k["xrecv"].at[xi, half]
-            start(src, dst, sem("rx", xi, half), where)
+        total = whole(xi)
+        for yi in (3, 2, 1, 0):
+            if xi or yi:
+                k["xsend"][xi, yi] = total[yi * 16 : yi * 16 + 16].astype(BF)
+                where = {"y": lax.rem(y - XORD[yi] + NY, NY), "x": lax.rem(x - XORD[xi] + NX, NX)}
+                start(k["xsend"].at[xi, yi], k["xrecv"].at[xi, yi], sem("rx", xi, yi), where)
+        return total[:16]
 
     for xi in range(3):
         to_rows(xi)
     up(0, 192)
     with jax.named_scope("w_dxl"):
-        for yi in range(NY):
-            await_recv(part_of(3, yi, 0), sem("dl", 0, yi), {"tp": other})
-        send_core(3, 0)
-        for yi in range(NY):
-            wait_x(2, yi, 1)
-        send_core(3, 1)
+        for g in range(2):
+            for yi in range(NY):
+                wait_plane(3, yi, g)
+            send_core(3, g)
     down(1)
     down(2)
     to_rows(3)
@@ -557,29 +544,18 @@
     send_sum(2)
     send_sum(3)
     down(0)
-    home = whole(0)
+    home = send_sum(0)
     back = iota(square, 0) == iota(square, 1) % 16 * Q + iota(square, 1) // 16
     back = jnp.where(back, 1.0, 0.0).astype(BF)
     for half in (1, 0):
-        with jax.named_scope(f"w_rx{half}"):
-            for n in range(1, 4):
-                await_recv(k["xrecv"].at[n, half], sem("rx", n, half), {"tp": other})
-        rows = home[half * 32 : half * 32 + 32]
-        rows = sum((k["xrecv"][n, half].astype(F32) for n in range(1, 4)), rows).astype(BF)
-        for yi in (3, 2) if half else (1, 0):
-            part = rows[yi % 2 * 16 : yi % 2 * 16 + 16]
-            part = jnp.concatenate([part[:, q * LANES : (q + 1) * LANES] for q in range(Q)], axis=0)
-            part = dot(back, part).astype(BF).reshape(NZ, 16, LANES)
-            if yi:
-                k["ysend"][yi] = part
-                where = {"y": lax.rem(y - XORD[yi] + NY, NY)}
-                start(k["ysend"].at[yi], k["ry"].at[yi], sem("ry", yi), where)
-            else:
-                k["ry"][0] = part
-    for half in (1, 0):
-        with jax.named_scope(f"w_ry{half}"):
-            for yi in (2, 3) if half else (1,):
-                await_recv(k["ry"].at[yi], sem("ry", yi), {"tp": other})
+        for yi in (2 * half + 1, 2 * half):
+            with jax.named_scope(f"w_rx{yi}"):
+                for xi in range(0 if yi else 1, NX):
+                    await_recv(k["xrecv"].at[xi, yi], sem("rx", xi, yi), {"tp": other})
+            rows = sum(k["xrecv"][xi, yi].astype(F32) for xi in range(1, NX))
+            rows = (rows + (k["xrecv"][0, yi].astype(F32) if yi else home)).astype(BF)
+            part = jnp.concatenate([rows[:, q * LANES : (q + 1) * LANES] for q in range(Q)], axis=0)
+            k["ry"][yi] = dot(back, part).astype(BF).reshape(NZ, 16, LANES)
         pair = pl.ds(2 * half, 2)
         for i in range(7, 0, -1):
             there = lax.rem(z - ZORD[i] + NZ, NZ)
@@ -597,6 +573,10 @@
     mix = dot(k["pw"][...], returned, ((0,), (0,)), HIGHEST)
     expert_mix = jnp.concatenate([mix[q * S : (q + 1) * S] for q in range(Q)], axis=1)
     o_stream[...] = (mid_values + expert_mix).astype(BF)
+    for n in range(2):
+        for d in range(8):
+            ref = k["wo"].at[x, 0]
+            remote(ref, ref, k["spread"].at[n, d], sem("ox", n, d), {"tp": other}).wait_send()
     for c in sent[-SENDS:]:
         c.wait_send()
     sends_done("ss", "ra", "a_s", "a_r")

time: 76.3 us -> 72.1 us (0.945)
  Pallas kernels: 75.6 us -> 71.3 us
    pallas_call x1, Pallas kernels: 73.9 us -> 69.7 us  [per_device(): pl.pallas_call(kernel, name='layer', out_shape=(jax.ShapeDtypeStruct((S,...]
where the time goes in v5:
time: 72.1 us; the launch traced here: 71.9 us
  Pallas kernels  71.3 us (99%)
    pallas_call x1, Pallas kernels, per_device(): pl.pallas_call(kernel, name='layer', out_shape=(jax.ShapeDtypeStruct((S,...  69.7 us
    pallas_call x1, Pallas kernels, per_device(): pl.pallas_call(handed_on, name='handed_on', out_shape=tuple((jax.ShapeDty...  1.63 us

profile of v5, /device:TPU:2, one launch (start us, length us, event | category | flops | bytes accessed | tf_op | source)
XLA Modules:
  0.0 71.9 jit_solution(5912463336181728069)
XLA Ops:
  0.6 69.7 %layer.1 = (bf16[16,1024]{1,0:T(8,128)(2,1)}, f32[16,1024]{1,0:T(8,128)}, bf16[3,16,1024]{2,1,0:T(8,128)(2,1)}) custom-call(bf16[16,1024]{1,0:T(8,128)(2,1)} %refs_0_.1, f32[16,1024]{1,0:T(8,128)} %refs_1_.1, bf16[3,16,1024]{2,1,0:T(8,128)(2,1)} %bitcast.18, f32[1,1024]{1,0:T(1,128)} %bitcast.22, bf16[16,1024]{1,0:T(8,128)(2,1)} %bitcast.19, ...), custom_call_target="tpu_custom_call" | custom-call | tf_op jit(solution)/shard_map/layer/pallas_call | solution.py:597
  70.3 1.6 %handed_on.1 = (bf16[16,1024]{1,0:T(8,128)(2,1)}, f32[16,1024]{1,0:T(8,128)}, bf16[3,16,1024]{2,1,0:T(8,128)(2,1)}) custom-call(bf16[16,1024]{1,0:T(8,128)(2,1)} %get-tuple-element.9.refs_0_, f32[16,1024]{1,0:T(8,128)} %get-tuple-element.10.refs_1_, bf16[3,16,1024]{2,1,0:T(8,128)(2,1)} %get-tuple-element.11.refs_2_), custom_call_target="tpu_custom_call" | custom-call | tf_op jit(solution)/shard_map/handed_on/pallas_call | solution.py:630

commit v6 on v5

--- a/solution.py
+++ b/solution.py
@@ -539,9 +539,9 @@
     down(2)
     to_rows(3)
     up(192, 256)
-    down(3)
     send_sum(1)
     send_sum(2)
+    down(3)
     send_sum(3)
     down(0)
     home = send_sum(0)

time: 72.1 us -> 71.6 us (level)
  no operation moved by 1% of the time
where the time goes in v6:
time: 71.6 us; the launch traced here: 71.5 us
  Pallas kernels  70.8 us (99%)
    pallas_call x1, Pallas kernels, per_device(): pl.pallas_call(kernel, name='layer', out_shape=(jax.ShapeDtypeStruct((S,...  69.2 us
    pallas_call x1, Pallas kernels, per_device(): pl.pallas_call(handed_on, name='handed_on', out_shape=tuple((jax.ShapeDty...  1.63 us

profile of v6, /device:TPU:2, one launch (start us, length us, event | category | flops | bytes accessed | tf_op | source)
XLA Modules:
  0.0 71.5 jit_solution(2379691339987639954)
XLA Ops:
  0.6 69.2 %layer.1 = (bf16[16,1024]{1,0:T(8,128)(2,1)}, f32[16,1024]{1,0:T(8,128)}, bf16[3,16,1024]{2,1,0:T(8,128)(2,1)}) custom-call(bf16[16,1024]{1,0:T(8,128)(2,1)} %refs_0_.1, f32[16,1024]{1,0:T(8,128)} %refs_1_.1, bf16[3,16,1024]{2,1,0:T(8,128)(2,1)} %bitcast.18, f32[1,1024]{1,0:T(1,128)} %bitcast.22, bf16[16,1024]{1,0:T(8,128)(2,1)} %bitcast.19, ...), custom_call_target="tpu_custom_call" | custom-call | tf_op jit(solution)/shard_map/layer/pallas_call | solution.py:597
  69.8 1.6 %handed_on.1 = (bf16[16,1024]{1,0:T(8,128)(2,1)}, f32[16,1024]{1,0:T(8,128)}, bf16[3,16,1024]{2,1,0:T(8,128)(2,1)}) custom-call(bf16[16,1024]{1,0:T(8,128)(2,1)} %get-tuple-element.9.refs_0_, f32[16,1024]{1,0:T(8,128)} %get-tuple-element.10.refs_1_, bf16[3,16,1024]{2,1,0:T(8,128)(2,1)} %get-tuple-element.11.refs_2_), custom_call_target="tpu_custom_call" | custom-call | tf_op jit(solution)/shard_map/handed_on/pallas_call | solution.py:630

commit v7 on v6

--- a/solution.py
+++ b/solution.py
@@ -10,7 +10,7 @@
 EP_TP = ("z", "y", "x", "tp")
 MESH = pl.DeviceIdType.MESH
 NZ, NY, NX = 8, 4, 4
-ORDER = {8: (4, 3, 5, 2, 6, 1, 7), 4: (2, 1, 3)}
+ORDER = {8: (1, 7, 2, 6, 3, 5, 4), 4: (2, 1, 3)}
 ZORD, XORD = (0, 1, 7, 2, 6, 3, 5, 4), (0, 1, 3, 2)
 GROUPS = ((0, 5), (5, 3))
 PLANE = tuple((i, j) for i in (3, 2, 1, 0) for j in (3, 2, 1, 0) if i or j)

time: 71.6 us -> 72.7 us (1.015)
  the two profiles are of different devices: /device:TPU:2 before, /device:TPU:1 now
where the time goes in v7:
time: 72.7 us; the launch traced here: 72.6 us
  Pallas kernels  72 us (99%)
    pallas_call x1, Pallas kernels, per_device(): pl.pallas_call(kernel, name='layer', out_shape=(jax.ShapeDtypeStruct((S,...  70.4 us
    pallas_call x1, Pallas kernels, per_device(): pl.pallas_call(handed_on, name='handed_on', out_shape=tuple((jax.ShapeDty...  1.63 us

profile of v7, /device:TPU:1, one launch (start us, length us, event | category | flops | bytes accessed | tf_op | source)
XLA Modules:
  0.0 72.6 jit_solution(6157459427915974867)
XLA Ops:
  0.6 70.4 %layer.1 = (bf16[16,1024]{1,0:T(8,128)(2,1)}, f32[16,1024]{1,0:T(8,128)}, bf16[3,16,1024]{2,1,0:T(8,128)(2,1)}) custom-call(bf16[16,1024]{1,0:T(8,128)(2,1)} %refs_0_.1, f32[16,1024]{1,0:T(8,128)} %refs_1_.1, bf16[3,16,1024]{2,1,0:T(8,128)(2,1)} %bitcast.18, f32[1,1024]{1,0:T(1,128)} %bitcast.22, bf16[16,1024]{1,0:T(8,128)(2,1)} %bitcast.19, ...), custom_call_target="tpu_custom_call" | custom-call | tf_op jit(solution)/shard_map/layer/pallas_call | solution.py:597
  71.0 1.6 %handed_on.1 = (bf16[16,1024]{1,0:T(8,128)(2,1)}, f32[16,1024]{1,0:T(8,128)}, bf16[3,16,1024]{2,1,0:T(8,128)(2,1)}) custom-call(bf16[16,1024]{1,0:T(8,128)(2,1)} %get-tuple-element.9.refs_0_, f32[16,1024]{1,0:T(8,128)} %get-tuple-element.10.refs_1_, bf16[3,16,1024]{2,1,0:T(8,128)(2,1)} %get-tuple-element.11.refs_2_), custom_call_target="tpu_custom_call" | custom-call | tf_op jit(solution)/shard_map/handed_on/pallas_call | solution.py:630
